TPU v7x, 128 devices: a whole 4x4x4 slice. The times are simulated.
128 devices in a mesh: sp: 64 (over z, y, x), tp: 2 (over core).
Axes of the slice: x: 4, y: 4, z: 4, core: 2. Of those that a mesh axis runs over, the one named last changes fastest.
Arguments:
- residual: bfloat16 [16384, 2048], P(('sp', 'tp')), may hold values from -6 to 6
- query_one: bfloat16 [16384, 512], P('sp', 'tp'), may hold values from -6.5 to 6.5
- key_one: bfloat16 [16384, 512], P('sp', 'tp'), may hold values from -6.5 to 6.5
- query_two: bfloat16 [16384, 512], P('sp', 'tp'), may hold values from -6.5 to 6.5
- key_two: bfloat16 [16384, 512], P('sp', 'tp'), may hold values from -6.5 to 6.5
- value_rows: bfloat16 [16384, 1024], P('sp', 'tp'), may hold values from -6 to 6
- lambda_head: float32 [8], P('tp'), may hold values from 0.3 to 0.8
- head_gain: float32 [128], replicated, may hold values from 0.1 to 1.9
- out_weight: bfloat16 [1024, 2048], replicated, may hold values from -0.1875 to 0.1875
- norm_gain: float32 [2048], replicated, may hold values from 0.1 to 1.9
- route_ids: int32 [16384, 2], P(('sp', 'tp')), may hold values from 0 to 63, all different within a row; in each aligned block of 128 rows (0 to 127, 128 to 255, ...) at most 6 rows name the same one
- route_weights: float32 [16384, 2], P(('sp', 'tp')), may hold values from 0.25 to 1
- gate_weight: bfloat16 [64, 2048, 512], P('sp', None, 'tp'), may hold values from -0.125 to 0.125
- up_weight: bfloat16 [64, 2048, 512], P('sp', None, 'tp'), may hold values from -0.125 to 0.125
- down_weight: bfloat16 [64, 512, 2048], P('sp', 'tp'), may hold values from -0.25 to 0.25
Outputs:
- mixed: bfloat16 [16384, 2048], P(('sp', 'tp'))
Inputs may be any that keep to these rules, and one draw needn't show every extreme that they name: `route_ids`: each row names 2 different experts. Among the rows of one device (aligned blocks of 128 rows) no expert is named more than 6 times, and in every draw some device has an expert named exactly 6 times.
All inputs are finite; a program needn't handle non-finite values.
Results may differ from a plain program's by a relative error of at most 0.014.
Values may be sent and summed in bfloat16 or wider, within the bound.
A program may use at most 128 MiB of HBM per device.

v0:
```python
import jax
import jax.numpy as jnp
from jax import lax
from jax.sharding import PartitionSpec as P

epsilon = 1e-06
low_value = -1e30


def sent_together(arrays, axis, dim, along):
    ends, at = ([], 0)
    for a in arrays[:-1]:
        at += a.shape[along]
        ends.append(at)
    both = jnp.concatenate(arrays, axis=along)
    return tuple(jnp.split(lax.all_gather(both, axis, axis=dim, tiled=True), ends, axis=along))


def cut_along(x, dim, size):
    lengths = x.shape
    blocks = x.reshape(*lengths[:dim], size, lengths[dim] // size, *lengths[dim + 1 :])
    return jnp.moveaxis(blocks, dim, 0)


def summed_on_arrival(x, axis, dim):
    size = lax.axis_size(axis)
    blocks = lax.all_to_all(cut_along(x, dim, size), axis, 0, 0, tiled=True)
    return jnp.sum(blocks.astype(jnp.float32), axis=0)


def online_update(carried, queries, keys_block, values_block, query_pos, key_pos, score_scale):
    running_max, running_sum, summed = carried
    scores = (
        jnp.einsum("qhd,khd->qhk", queries, keys_block, preferred_element_type=jnp.float32)
        * score_scale
    )
    allowed = (query_pos[:, None] >= key_pos[None, :])[:, None, :]
    scores = jnp.where(allowed, scores, low_value)
    newest = jnp.maximum(running_max, jnp.max(scores, axis=-1))
    exp_weights = jnp.where(allowed, jnp.exp(scores - newest[..., None]), 0.0)
    factor = jnp.exp(running_max - newest)
    running_sum = running_sum * factor + jnp.sum(exp_weights, axis=-1)
    product = jnp.einsum(
        "qhk,khd->qhd",
        exp_weights.astype(jnp.bfloat16),
        values_block,
        preferred_element_type=jnp.float32,
    )
    summed = summed * factor[..., None] + product
    return (newest, running_sum, summed)


def expert_rows(rows, gate_half, up_half, down_half):
    gate = jnp.dot(rows, gate_half, preferred_element_type=jnp.float32)
    upper = jnp.dot(rows, up_half, preferred_element_type=jnp.float32)
    hidden = (jax.nn.silu(gate) * upper).astype(jnp.bfloat16)
    return jnp.dot(hidden, down_half, preferred_element_type=jnp.float32)


def on_device(
    residual,
    query_one,
    key_one,
    query_two,
    key_two,
    value_rows,
    lambda_head,
    head_gain,
    out_weight,
    norm_gain,
    route_ids,
    route_weights,
    gate_weight,
    up_weight,
    down_weight,
):
    row_count = query_one.shape[0]
    head_count = lambda_head.shape[0]
    head_dim = query_one.shape[1] // head_count
    value_dim = value_rows.shape[1] // head_count
    model_width = residual.shape[1]
    tp_count = lax.axis_size("tp")
    sp_count = lax.axis_size("sp")
    score_scale = head_dim ** (-0.5)
    offset = lax.axis_index("sp") * row_count
    query_pos = offset + jnp.arange(row_count)
    last_query = offset + row_count - 1
    first_query = query_one.reshape(row_count, head_count, head_dim)
    second_query = query_two.reshape(row_count, head_count, head_dim)
    empty_state = (
        jnp.full((row_count, head_count), low_value, jnp.float32),
        jnp.zeros((row_count, head_count), jnp.float32),
        jnp.zeros((row_count, head_count, value_dim), jnp.float32),
    )
    pieces = sent_together((key_one, key_two, value_rows), "sp", 0, 1)
    piece_rows = pieces[0].shape[0]
    width_block = 512

    def one_block(position, inner_state):
        begin_row = position * width_block

        def advance(current):
            first_keys = lax.dynamic_slice_in_dim(pieces[0], begin_row, width_block, 0).reshape(
                width_block, head_count, head_dim
            )
            second_keys = lax.dynamic_slice_in_dim(pieces[1], begin_row, width_block, 0).reshape(
                width_block, head_count, head_dim
            )
            value_part = lax.dynamic_slice_in_dim(pieces[2], begin_row, width_block, 0).reshape(
                width_block, head_count, value_dim
            )
            key_pos = begin_row + jnp.arange(width_block)
            first_next = online_update(
                current[0], first_query, first_keys, value_part, query_pos, key_pos, score_scale
            )
            second_next = online_update(
                current[1], second_query, second_keys, value_part, query_pos, key_pos, score_scale
            )
            return (first_next, second_next)

        return lax.cond(begin_row <= last_query, advance, lambda unchanged: unchanged, inner_state)

    first_state, second_state = lax.fori_loop(
        0, piece_rows // width_block, one_block, (empty_state, empty_state)
    )
    first_out = first_state[2] / first_state[1][..., None]
    second_out = second_state[2] / second_state[1][..., None]
    head_out = first_out - lambda_head[None, :, None] * second_out
    normed = (
        head_out
        * lax.rsqrt(jnp.mean(head_out * head_out, axis=-1, keepdims=True) + epsilon)
        * head_gain
    )
    attended = normed.reshape(row_count, head_count * value_dim).astype(jnp.bfloat16)
    own_width = attended.shape[1]
    own_rows = lax.dynamic_slice_in_dim(out_weight, lax.axis_index("tp") * own_width, own_width, 0)
    projected = summed_on_arrival(
        jnp.dot(attended, own_rows, preferred_element_type=jnp.float32).astype(jnp.bfloat16),
        "tp",
        0,
    )
    after_float = (
        (residual.astype(jnp.float32) + projected).astype(jnp.bfloat16).astype(jnp.float32)
    )
    routed = (
        after_float
        * lax.rsqrt(jnp.mean(after_float * after_float, axis=-1, keepdims=True) + epsilon)
        * norm_gain
    ).astype(jnp.bfloat16)
    local_rows, top_count = route_ids.shape
    expert_count = gate_weight.shape[0] * sp_count
    capacity = max(2, (3 * row_count + 2 * sp_count - 1) // (2 * sp_count))
    flat_ids = route_ids.reshape(-1)
    onehot = (flat_ids[:, None] == jnp.arange(expert_count)[None, :]).astype(jnp.int32)
    rank = jnp.sum((jnp.cumsum(onehot, axis=0) - onehot) * onehot, axis=1)
    slot = flat_ids * capacity + rank
    source_row = jnp.arange(local_rows * top_count) // top_count
    slot_rows = jnp.full((expert_count * capacity,), -1, jnp.int32).at[slot].set(source_row)
    filled = (slot_rows >= 0)[:, None]
    outgoing = jnp.where(filled, routed[jnp.maximum(slot_rows, 0)], jnp.zeros((), jnp.bfloat16))
    outgoing = outgoing.reshape(expert_count, capacity, model_width)
    gate_half = gate_weight[0]
    up_half = up_weight[0]
    down_half = down_weight[0]
    doubled = jnp.broadcast_to(outgoing[:, None], (expert_count, tp_count, capacity, model_width))
    doubled = doubled.reshape(expert_count * tp_count, capacity, model_width)
    arrived = lax.all_to_all(doubled, ("sp", "tp"), split_axis=0, concat_axis=0, tiled=True)
    sources, items, width_rows = arrived.shape
    partial_value = expert_rows(
        arrived.reshape(sources * items, width_rows), gate_half, up_half, down_half
    )
    partial_value = partial_value.reshape(sources // tp_count, tp_count, items, width_rows)
    summed = summed_on_arrival(partial_value.astype(jnp.bfloat16), "tp", 1).astype(jnp.bfloat16)
    summed = summed.reshape(sources // tp_count, items, width_rows)
    returned = lax.all_to_all(summed, "sp", split_axis=0, concat_axis=0, tiled=True)
    flat_back = returned.reshape(expert_count * capacity, model_width)
    picked = flat_back[slot].astype(jnp.float32).reshape(local_rows, top_count, model_width)
    moe_out = jnp.sum(picked * route_weights[..., None], axis=1)
    return (after_float + moe_out).astype(jnp.bfloat16)


def solution(mesh):
    placed = (
        P(("sp", "tp"), None),
        P("sp", "tp"),
        P("sp", "tp"),
        P("sp", "tp"),
        P("sp", "tp"),
        P("sp", "tp"),
        P("tp"),
        P(),
        P(),
        P(),
        P(("sp", "tp"), None),
        P(("sp", "tp"), None),
        P("sp", None, "tp"),
        P("sp", None, "tp"),
        P("sp", "tp", None),
    )
    return jax.shard_map(
        on_device, mesh=mesh, in_specs=placed, out_specs=P(("sp", "tp"), None), check_vma=False
    )
```

profile of v0, /device:TPU:2, one launch (start us, length us, event | category | flops | bytes accessed | tf_op | source)
XLA Modules:
  0.0 646.5 jit_solution(14021550046197942882)
XLA Ops:
  6.5 0.0 all-gather.2.cloned.1.call-start
  6.6 1.2 copy.58
  7.8 1.0 copy.56
  8.8 1.0 copy.57
  9.8 0.8 pad_maximum_fusion
  10.6 0.0 all-gather.2.cloned.1.call-update
  10.7 0.1 copy.62
  10.8 0.1 eq.29
  10.9 0.1 eq.25
  11.1 0.1 copy.59
  11.2 0.1 copy.60
  11.3 0.6 reduce-window.6
  11.9 0.2 slice_reduce_fusion
  12.1 0.1 copy.61
  12.3 0.1 mul.138
  12.4 0.1 fusion.40
  12.5 1.4 scatter_custom_fusion
  14.0 0.1 broadcast_in_dim.86
  14.1 225.7 %all-gather.2.cloned.1.call-done = bf16[16384,1024]{0,1:T(8,128)(2,1)} async-done(((bf16[256,1024]{0,1:T(8,128)(2,1)}), bf16[16384,1024]{0,1:T(8,128)(2,1)}) %all-gather.2.cloned.1.call-update) | async-done | bytes 33554448 | tf_op jit(solution)/shard_map/all_gather | solution.py:16
  239.8 13.2 %fusion.45 = (bf16[16384,256]{0,1:T(8,128)(2,1)}, bf16[16384,256]{0,1:T(8,128)(2,1)}) fusion(bf16[16384,1024]{0,1:T(8,128)(2,1)} %all-gather.2.cloned.1.call-done), kind=kLoop, calls=%fused_computation.93 | loop fusion | bytes 33554432 | tf_op jit(solution)/shard_map/split | solution.py:16
  253.0 8.1 %copy-done.1 = bf16[16384,1024]{0,1:T(8,128)(2,1)S(1)} copy-done((bf16[16384,1024]{0,1:T(8,128)(2,1)S(1)}, bf16[16384,1024]{0,1:T(8,128)(2,1)}, u32[]{:S(2)}) %copy-start.1) | copy-done | bytes 33554456
  261.1 6.6 %split.13 = bf16[16384,512]{0,1:T(8,128)(2,1)} slice(bf16[16384,1024]{0,1:T(8,128)(2,1)S(1)} %copy-done.1), slice={[0:16384], [512:1024]} | slice | bytes 33554432 | tf_op jit(solution)/shard_map/split | solution.py:16
  267.8 0.0 copy-start.12
  267.8 8.9 %while.24 = (s32[]{:T(128)}, f32[256,4]{0,1:T(4,128)S(1)}, f32[256,4]{0,1:T(4,128)S(1)}, f32[256,4,128]{0,2,1:T(8,128)S(1)}, f32[256,4]{0,1:T(4,128)S(1)}, /*ind...) while((s32[]{:T(128)}, f32[256,4]{0,1:T(4,128)S(1)}, ...), condition=%wide.region_7.8_spmd.clone, body=%wide.region_0.7_spmd.clone.sunk | while | flops 416944896 | bytes 21504444 | solution.py:123
  267.9 7.1 %conditional.3 = ((f32[256,4]{0,1:T(4,128)S(1)}, f32[256,4]{0,1:T(4,128)S(1)}, f32[256,4,128]{0,2,1:T(8,128)S(1)}, f32[256,4]{0,1:T(4,128)S(1)}, f32[256,4]{0,1:T(4,128)S(1)}, /*index=5*/f32[256,4,128]{0,2,1:T(8,128)S(1)})) conditional(s32[]{:T(128)} %convert_element_type.110, (f32[256,4]{0,1:T(4,128)S(1)}, f32[256,4]{0,1:T(4,128)S(1)}, ...), branch_computations={%region_1.0_spmd, %region_2.6_spmd} | conditional | flops 416944896 | bytes 21503086 | solution.py:121
  267.9 1.0 constant_dynamic-slice_fusion.2
  268.9 0.5 fusion.46
  269.4 1.0 constant_dynamic-slice_fusion
  270.4 0.1 broadcast_compare_fusion
  270.5 0.7 fusion.3
  271.3 1.0 fusion.7
  272.3 1.1 constant_dynamic-slice_fusion.1
  273.4 0.8 fusion.8
  274.2 0.7 fusion.9
  276.8 0.2 multiply_reduce_fusion.1
  277.0 0.1 multiply_convert_fusion
  277.1 2.3 convolution_convert_fusion.1
  279.5 4.7 all_to_all.20
  284.2 0.2 convert_reduce_fusion
  284.4 0.3 fusion.29
  284.7 0.8 copy-done.2
  285.5 0.2 fusion.31
  285.7 3.1 gather_fusion
  288.8 2.5 gather.9
  291.3 0.3 broadcast_select_fusion
  291.6 0.5 broadcast_in_dim.90
  292.1 279.1 %all_to_all.21 = bf16[128,6,2048]{2,1,0:T(8,128)(2,1)} all-to-all(bf16[128,6,2048]{2,1,0:T(8,128)(2,1)S(1)} %bitcast.91), channel_id=1, replica_groups=mesh['sp'=64,'tp'=2] {'sp','tp'}, dimensions={0} | all-to-all | bytes 6291456 | tf_op jit(solution)/shard_map/all_to_all | solution.py:167
  571.2 6.4 reshape.158
  577.7 3.0 fusion.35
  580.7 0.1 copy-done.14
  580.8 1.0 fusion.28
  581.8 0.1 dot_general.29
  581.9 1.0 fusion.26
  582.9 6.3 all_to_all.22
  589.2 0.7 bitcast_reduce_fusion
  589.9 2.2 copy.68
  592.1 6.5 %all-to-all-start.3 = ((bf16[64,6,2048]{2,1,0:T(8,128)(2,1)}), bf16[64,6,2048]{2,1,0:T(8,128)(2,1)}, u32[]{:S(2)}, u32[]{:S(2)}) async-start(bf16[64,6,2048]{2,1,0:T(8,128)(2,1)} %copy.68), calls=%async_computation.3 | async-start | bytes 4194304 | tf_op jit(solution)/shard_map/all_to_all | solution.py:175
  598.6 0.1 copy.69
  598.7 29.6 %all-to-all-done.3 = bf16[64,6,2048]{2,1,0:T(8,128)(2,1)} async-done(((bf16[64,6,2048]{2,1,0:T(8,128)(2,1)}), bf16[64,6,2048]{2,1,0:T(8,128)(2,1)}, u32[]{:S(2)}, u32[]{:S(2)}) %all-to-all-start.3) | async-done | bytes 1572896 | tf_op jit(solution)/shard_map/all_to_all | solution.py:175
  628.3 2.6 reshape.160
  630.9 2.3 gather_fusion.1
  633.2 2.4 reshape.161
  635.6 3.2 multiply_reduce_fusion
  638.8 0.9 fusion.32
  (114 shorter events, 0.8 us)
Async XLA Ops:
  6.5 575.4 %copy-start = (bf16[1,256,2048]{2,1,0:T(8,128)(2,1)S(1)}, bf16[1,256,2048]{2,1,0:T(8,128)(2,1)}, u32[]{:S(2)}) copy-start(bf16[1,256,2048]{2,1,0:T(8,128)(2,1)} %param.33) | copy-start | bytes 3145732
  6.5 4.1 copy-start.9
  6.5 4.5 copy-start.6
  6.5 4.6 copy-start.7
  6.5 233.3 %all-gather.2.cloned.1.call-start = ((), (), s32[]{:S(2)}) async-start(), calls=%async_computation.4 | async-start | bytes 34078720 | tf_op jit(solution)/shard_map/all_gather | solution.py:16
  239.8 21.3 %copy-start.1 = (bf16[16384,1024]{0,1:T(8,128)(2,1)S(1)}, bf16[16384,1024]{0,1:T(8,128)(2,1)}, u32[]{:S(2)}) copy-start(bf16[16384,1024]{0,1:T(8,128)(2,1)} %all-gather.2.cloned.1.call-done) | copy-start | bytes 100663296
  267.8 9.0 %copy-start.11 = (f32[4]{0:T(128)S(1)}, f32[4]{0:T(128)}, u32[]{:S(2)}) copy-start(f32[4]{0:T(128)} %param.25) | copy-start | bytes 52
  267.8 9.2 %copy-start.12 = (f32[128]{0:T(128)S(1)}, f32[128]{0:T(128)}, u32[]{:S(2)}) copy-start(f32[128]{0:T(128)} %param.26) | copy-start | bytes 1540
  279.5 4.9 copy-start.5
  284.2 1.3 copy-start.8
  284.7 0.8 copy-start.2
  571.2 6.4 copy-start.13
  577.7 3.0 copy-start.4
  577.7 3.1 copy-start.14
  592.1 6.5 %copy-start.10 = (f32[128,2]{0,1:T(2,128)S(1)}, f32[128,2]{0,1:T(2,128)}, u32[]{:S(2)}) copy-start(f32[128,2]{0,1:T(2,128)} %param.30) | copy-start | bytes 3076
  592.1 36.2 %all-to-all-start.3 = ((bf16[64,6,2048]{2,1,0:T(8,128)(2,1)}), bf16[64,6,2048]{2,1,0:T(8,128)(2,1)}, u32[]{:S(2)}, u32[]{:S(2)}) async-start(bf16[64,6,2048]{2,1,0:T(8,128)(2,1)} %copy.68), calls=%async_computation.3 | async-start | bytes 4194304 | tf_op jit(solution)/shard_map/all_to_all | solution.py:175
  635.6 3.2 copy-start.3
Sparse Core Ops, SparseCore 0:
  10.8 228.9 all-gather.1
where the time goes:
time: 652 us; the launch traced here: 647 us
  blocking collectives  290 us (44%)
  waiting for transfers between devices  255 us (39%)
  local copies, waits for them, and re-layouts  60.1 us (9%)
  between operations  13.8 us (2%)
  matrix products  10.1 us (2%)
  other arithmetic  8.8 us (1%)
  starting transfers between devices  6.53 us (1%)
    all_to_all x1, blocking collectives, on_device(): lax.all_to_all(doubled, ('sp', 'tp'), split_axis=0, concat_axis=0, tiled=...  279 us
    all_gather x1, waiting for transfers between devices, sent_together(): lax.all_gather(both, axis, axis=dim, tiled=True)  226 us
    all_to_all x1, waiting for transfers between devices, on_device(): lax.all_to_all(summed, 'sp', split_axis=0, concat_axis=0, tiled=True)  29.6 us
    split x2, local copies, waits for them, and re-layouts, sent_together(): jnp.split(lax.all_gather(both, axis, axis=dim, tiled=True), ends, axis=al...  19.8 us
  transfers between devices with their start and end apart: 2, of which 2 were waited for; matrix products, arithmetic and copies ran while one was open for 1% of the time, Pallas kernels for 0%

commit v1 on v0

v1 whole, which is shorter than its diff:
```python
import functools
import jax
import jax.numpy as jnp
from jax import lax
from jax.experimental import pallas as pl
from jax.experimental.pallas import tpu as pltpu
from jax.sharding import PartitionSpec as P

epsilon = 1e-06
low_value = -1e30
MESH = pl.DeviceIdType.MESH
ROWS = 256
CAP = 6
DIM_BITS = (1, 2, 4)
ORDERS = ((1, 2, 4), (2, 4, 1), (4, 1, 2), (1, 2, 4))


def to_class(p):
    return ((p + 1) // 2) % 2, p // 2


def to_coord(a, g):
    return 2 * g + (a + g) % 2


def sp_of(a, g):
    return to_coord(a[0], g[0]) * 16 + to_coord(a[1], g[1]) * 4 + to_coord(a[2], g[2])


def flipped(a, mask):
    return tuple((a[i] + ((mask >> (2 - i)) & 1)) % 2 for i in range(3))


class Place:
    def __init__(self):
        self.sp = lax.axis_index("sp")
        self.tp = lax.axis_index("tp")
        coords = (self.sp // 16, (self.sp // 4) % 4, self.sp % 4)
        pairs = [to_class(p) for p in coords]
        self.a = tuple(p[0] for p in pairs)
        self.g = tuple(p[1] for p in pairs)
        self.parity = (self.g[0] + self.g[1] + self.g[2]) % 2
        self.head = self.g[0] * 4 + self.g[1] * 2 + self.g[2]

    def source_g(self, j, core):
        gz, gy = j // 2, j % 2
        return (gz, gy, (core + gz + gy) % 2)


def remote(src, dst, send, recv, device):
    return pltpu.make_async_remote_copy(
        src_ref=src, dst_ref=dst, send_sem=send, recv_sem=recv, device_id=device, device_id_type=MESH
    )


def attention_kernel(
    kv_in, q_in, lam_in, gain_in, gate_in, up_in, down_in,
    att_out, gate_out, up_out, down_out,
    kv_all, q_all, lam_all, q_wide, acc, att_send, att_recv,
    s1_send, s1_recv, s2_send, s2_recv, sib_send, sib_recv, att_ssem, att_rsem, w_send, w_recv,
):
    me = Place()
    sibling = (me.sp, 1 - me.tp)
    barrier = pltpu.get_barrier_semaphore()
    count = 0
    for g in range(8):
        chip = sp_of(me.a, (g // 4, (g // 2) % 2, g % 2))
        for core in range(2):
            itself = (chip == me.sp) & (me.tp == core)

            @pl.when(jnp.logical_not(itself))
            def _():
                pl.semaphore_signal(barrier, inc=1, device_id=(chip, core), device_id_type=MESH)

            count += 1
    for bit in DIM_BITS:
        pl.semaphore_signal(
            barrier, inc=1, device_id=(sp_of(flipped(me.a, bit), me.g), me.tp), device_id_type=MESH
        )
        count += 1
    pl.semaphore_wait(barrier, count - 1)

    for hl in range(4):
        chip = sp_of(me.a, (me.tp, hl // 2, hl % 2))
        j = me.g[0] * 2 + me.g[1]
        itself = (chip == me.sp) & (me.parity == me.tp)
        parts = (
            (kv_in.at[hl], kv_all.at[me.sp]),
            (q_in.at[hl], q_all.at[j]),
            (lam_in.at[hl], lam_all.at[j]),
        )

        @pl.when(itself)
        def _():
            for n, (src, dst) in enumerate(parts):
                pltpu.make_async_copy(src, dst, s1_recv.at[n, j]).start()

        @pl.when(jnp.logical_not(itself))
        def _():
            for n, (src, dst) in enumerate(parts):
                remote(src, dst, s1_send.at[n, hl], s1_recv.at[n, j], (chip, me.parity)).start()

    weights = ((gate_in, gate_out), (up_in, up_out), (down_in, down_out))
    w_copies = [remote(a, b, w_send.at[n], w_recv.at[n], sibling) for n, (a, b) in enumerate(weights)]
    for c in w_copies:
        c.start()

    def tile(j, rel, core):
        return kv_all.at[sp_of(flipped(me.a, rel), me.source_g(j, core))]

    def hop(j, rel, bit):
        target = (sp_of(flipped(me.a, bit), me.g), me.tp)
        at = tile(j, rel, me.tp)
        return remote(at, at, s2_send.at[j, rel ^ bit], s2_recv.at[j, rel ^ bit], target)

    def across(j, rel):
        at = tile(j, rel, me.tp)
        return remote(at, at, sib_send.at[j, rel], sib_recv.at[j, rel], sibling)

    for j in range(4):
        pltpu.make_async_copy(q_all.at[j], q_all.at[j], s1_recv.at[1, j]).wait()
        pltpu.make_async_copy(lam_all.at[j], lam_all.at[j], s1_recv.at[2, j]).wait()
        at = tile(j, 0, me.tp)
        pltpu.make_async_copy(at, at, s1_recv.at[0, j]).wait()
        for bit in ORDERS[j]:
            hop(j, 0, bit).start()
        across(j, 0).start()
    for phase in range(3):
        for j in range(4):
            order = ORDERS[j]
            now = order[phase]
            earlier = [0]
            for b in order[:phase]:
                earlier += [r | b for r in earlier]
            for r in earlier:
                rel = r | now
                at = tile(j, rel, me.tp)
                pltpu.make_async_copy(at, at, s2_recv.at[j, rel]).wait()
                for b in order[phase + 1 :]:
                    hop(j, rel, b).start()
                across(j, rel).start()
    for j in range(4):
        for rel in range(8):
            at = tile(j, rel, 1 - me.tp)
            pltpu.make_async_copy(at, at, sib_recv.at[j, rel]).wait()

    for j in range(4):
        full = jnp.concatenate([q_all[j, 0:128, :], q_all[j, 128:256, :]], axis=1)
        row = lax.broadcasted_iota(jnp.int32, (128, 256), 0)
        zero = jnp.zeros_like(full)
        q_wide[j, :, 0:256] = jnp.where(row < 64, full, zero)
        q_wide[j, :, 256:512] = jnp.where(row >= 64, full, zero)

    wide = 2

    def one_tile(j, carry):
        gz, gy = j // 2, j % 2
        own = sp_of(me.a, (gz, gy, (me.tp + gz + gy) % 2))
        acc[...] = jnp.zeros_like(acc)

        def chunk(first, state, masked):
            m, l = state
            keys = jnp.concatenate([kv_all[first + i, 0:256, :] for i in range(wide)], axis=0)
            values = jnp.concatenate(
                [kv_all[first + i, 256 + 128 * b : 384 + 128 * b, :] for i in range(wide) for b in range(2)],
                axis=1,
            )
            s = jnp.dot(keys, q_wide[j], preferred_element_type=jnp.float32)
            if masked:
                key_pos = first * 256 + lax.broadcasted_iota(jnp.int32, s.shape, 0)
                q_pos = own * 256 + lax.broadcasted_iota(jnp.int32, s.shape, 1) % 256
                s = jnp.where(key_pos <= q_pos, s, low_value)
            newest = jnp.maximum(m, jnp.max(s, axis=0, keepdims=True))
            p = jnp.exp(s - newest)
            factor = jnp.exp(m - newest)
            l = l * factor + jnp.sum(p, axis=0, keepdims=True)
            acc[...] = acc[...] * factor + jnp.dot(
                values, p.astype(jnp.bfloat16), preferred_element_type=jnp.float32
            )
            return newest, l

        start = (jnp.full((1, 512), low_value, jnp.float32), jnp.zeros((1, 512), jnp.float32))
        whole = own // wide
        state = lax.fori_loop(0, whole, lambda i, st: chunk(i * wide, st, False), start)
        m, l = chunk(whole * wide, state, True)
        total = acc[...] / l
        for b in range(2):
            first = total[:, 128 * b : 128 * b + 128]
            second = total[:, 256 + 128 * b : 384 + 128 * b]
            out = first - lam_all[0, 0:1, :] * second
            mean = jnp.mean(out * out, axis=0, keepdims=True)
            out = out * lax.rsqrt(mean + epsilon) * gain_in[...]
            att_send[j, b] = out.astype(jnp.bfloat16)
        return carry

    lax.fori_loop(0, 4, one_tile, 0)

    for j in range(4):
        chip = sp_of(me.a, me.source_g(j, me.tp))
        for b in range(2):
            itself = (chip == me.sp) & (me.tp == b)

            @pl.when(itself)
            def _():
                pltpu.make_async_copy(att_send.at[j, b], att_recv.at[me.head], att_rsem.at[me.head]).start()

            @pl.when(jnp.logical_not(itself))
            def _():
                remote(
                    att_send.at[j, b], att_recv.at[me.head], att_ssem.at[j, b], att_rsem.at[me.head], (chip, b)
                ).start()

    for h in range(8):
        pltpu.make_async_copy(att_recv.at[h], att_recv.at[h], att_rsem.at[h]).wait()
        att_out[h] = att_recv[h]

    for j in range(4):
        chip = sp_of(me.a, me.source_g(j, me.tp))
        for b in range(2):

            @pl.when(jnp.logical_not((chip == me.sp) & (me.tp == b)))
            def _():
                pltpu.make_async_copy(att_send.at[j, b], att_send.at[j, b], att_ssem.at[j, b]).wait()

        for rel in range(8):
            if rel:
                at = tile(j, 0, me.tp)
                pltpu.make_async_copy(at, at, s2_send.at[j, rel]).wait()
            at = tile(j, rel, me.tp)
            pltpu.make_async_copy(at, at, sib_send.at[j, rel]).wait()
    for hl in range(4):
        chip = sp_of(me.a, (me.tp, hl // 2, hl % 2))

        @pl.when(jnp.logical_not((chip == me.sp) & (me.parity == me.tp)))
        def _():
            for n, src in enumerate((kv_in, q_in, lam_in)):
                pltpu.make_async_copy(src.at[hl], src.at[hl], s1_send.at[n, hl]).wait()

    for c in w_copies:
        c.wait()


def attention(kv, q, lam, gain, gate, up, down):
    vmem = pl.BlockSpec(memory_space=pltpu.VMEM)
    anywhere = pl.BlockSpec(memory_space=pl.ANY)
    dma = pltpu.SemaphoreType.DMA
    bf16 = jnp.bfloat16
    return pl.pallas_call(
        attention_kernel,
        out_shape=(
            jax.ShapeDtypeStruct((8, 128, 128), bf16),
            jax.ShapeDtypeStruct(gate.shape, bf16),
            jax.ShapeDtypeStruct(up.shape, bf16),
            jax.ShapeDtypeStruct(down.shape, bf16),
        ),
        in_specs=[vmem] * 4 + [anywhere] * 3,
        out_specs=(vmem, anywhere, anywhere, anywhere),
        scratch_shapes=[
            pltpu.VMEM((64, 512, 128), bf16),
            pltpu.VMEM((4, 256, 128), bf16),
            pltpu.VMEM((4, 8, 128), jnp.float32),
            pltpu.VMEM((4, 128, 512), bf16),
            pltpu.VMEM((128, 512), jnp.float32),
            pltpu.VMEM((4, 2, 128, 128), bf16),
            pltpu.VMEM((8, 128, 128), bf16),
            dma((3, 4)), dma((3, 4)), dma((4, 8)), dma((4, 8)), dma((4, 8)), dma((4, 8)),
            dma((4, 2)), dma((8,)), dma((3,)), dma((3,)),
        ],
        compiler_params=pltpu.CompilerParams(
            collective_id=0, has_side_effects=True, vmem_limit_bytes=40 * 1024 * 1024
        ),
    )(kv, q, lam, gain, gate, up, down)


def exchange_kernel(x, y, send, recv, local):
    sp = lax.axis_index("sp")
    tp = lax.axis_index("tp")
    z, yy, xx = sp // 16, (sp // 4) % 4, sp % 4

    def shifted(i, sign):
        dz, dy, dx = i // 16, (i // 4) % 4, i % 4
        return (
            ((z + sign * dz + 4) % 4) * 16 + ((yy + sign * dy + 4) % 4) * 4 + (xx + sign * dx + 4) % 4
        )

    barrier = pltpu.get_barrier_semaphore()

    @pl.loop(1, 64)
    def _(i):
        pl.semaphore_signal(barrier, inc=1, device_id=(shifted(i, 1), tp), device_id_type=MESH)

    mine = pltpu.make_async_copy(x.at[sp], y.at[sp], local)
    mine.start()
    pl.semaphore_wait(barrier, 63)

    def copy(i):
        to = shifted(i, 1)
        return remote(x.at[to], y.at[sp], send.at[i], recv.at[i], (to, tp))

    @pl.loop(1, 64)
    def _(i):
        copy(i).start()

    mine.wait()

    @pl.loop(1, 64)
    def _(i):
        at = y.at[shifted(i, -1)]
        pltpu.make_async_copy(at, at, recv.at[i]).wait()

    @pl.loop(1, 64)
    def _(i):
        copy(i).wait_send()


def exchange(x, number):
    anywhere = pl.BlockSpec(memory_space=pl.ANY)
    return pl.pallas_call(
        exchange_kernel,
        out_shape=jax.ShapeDtypeStruct(x.shape, x.dtype),
        in_specs=[anywhere],
        out_specs=anywhere,
        scratch_shapes=[
            pltpu.SemaphoreType.DMA((64,)), pltpu.SemaphoreType.DMA((64,)), pltpu.SemaphoreType.DMA
        ],
        compiler_params=pltpu.CompilerParams(collective_id=number, has_side_effects=True),
        name=f"exchange{number}",
    )(x)


def expert_hidden(rows, gate_half, up_half):
    gate = jnp.dot(rows, gate_half, preferred_element_type=jnp.float32)
    upper = jnp.dot(rows, up_half, preferred_element_type=jnp.float32)
    return (jax.nn.silu(gate) * upper).astype(jnp.bfloat16)


def on_device(
    residual, query_one, key_one, query_two, key_two, value_rows, lambda_head, head_gain, out_weight,
    norm_gain, route_ids, route_weights, gate_weight, up_weight, down_weight,
):
    rows = query_one.shape[0]
    width = residual.shape[1]
    scale = 64 ** (-0.5)

    def by_head(x, size):
        return x.reshape(rows, 4, size)

    keys = jnp.concatenate([by_head(key_one, 64), by_head(key_two, 64)], axis=2).transpose(1, 0, 2)
    values = value_rows.reshape(2, 128, 4, 128).transpose(2, 0, 3, 1).reshape(4, 256, 128)
    kv = jnp.concatenate([keys, values], axis=1)
    queries = jnp.concatenate([by_head(query_one, 64), by_head(query_two, 64)], axis=2) * jnp.bfloat16(scale)
    q = queries.reshape(2, 128, 4, 128).transpose(2, 0, 3, 1).reshape(4, 256, 128)
    lam = jnp.broadcast_to(lambda_head[:, None, None], (4, 8, 128))
    gain = jnp.broadcast_to(head_gain[:, None], (128, 128))
    attended, gate_other, up_other, down_other = attention(
        kv, q, lam, gain, gate_weight, up_weight, down_weight
    )
    attended = attended.reshape(1024, 128)
    projected = lax.dot_general(
        attended, out_weight, (((0,), (0,)), ((), ())), preferred_element_type=jnp.float32
    )
    after = (residual.astype(jnp.float32) + projected).astype(jnp.bfloat16)
    after_float = after.astype(jnp.float32)
    routed = (
        after_float
        * lax.rsqrt(jnp.mean(after_float * after_float, axis=-1, keepdims=True) + epsilon)
        * norm_gain
    ).astype(jnp.bfloat16)

    local = residual.shape[0]
    expert = jnp.arange(64)[:, None]
    first_hit = route_ids[:, 0][None, :] == expert
    second_hit = route_ids[:, 1][None, :] == expert
    hit = (first_hit | second_hit).astype(jnp.bfloat16)
    before = (jnp.arange(local)[:, None] < jnp.arange(local)[None, :]).astype(jnp.bfloat16)
    rank = jnp.dot(hit, before, preferred_element_type=jnp.float32)
    chosen = (rank[:, None, :] == jnp.arange(CAP, dtype=jnp.float32)[None, :, None]) & (hit[:, None, :] > 0)
    share = (
        jnp.where(first_hit, route_weights[:, 0][None, :], 0.0)
        + jnp.where(second_hit, route_weights[:, 1][None, :], 0.0)
    )
    pick = chosen.astype(jnp.bfloat16).reshape(64 * CAP, local)
    blend = jnp.where(chosen, share[:, None, :], 0.0).reshape(64 * CAP, local)
    blend_high = lax.reduce_precision(blend, 8, 7)
    blend_low = blend - blend_high

    outgoing = jnp.dot(pick, routed, preferred_element_type=jnp.float32).astype(jnp.bfloat16)
    arrived = exchange(outgoing.reshape(64, CAP // 2, 2, width), 1).reshape(64 * CAP, width)
    own = expert_hidden(arrived, gate_weight[0], up_weight[0])
    other = expert_hidden(arrived, gate_other[0], up_other[0])
    made = jnp.dot(own, down_weight[0], preferred_element_type=jnp.float32) + jnp.dot(
        other, down_other[0], preferred_element_type=jnp.float32
    )
    returned = exchange(made.astype(jnp.bfloat16).reshape(64, CAP // 2, 2, width), 2)
    returned = returned.reshape(64 * CAP, width)
    dims = (((0,), (0,)), ((), ()))
    moe_out = lax.dot_general(
        blend_high.astype(jnp.bfloat16), returned, dims, preferred_element_type=jnp.float32
    ) + lax.dot_general(
        blend_low.astype(jnp.bfloat16), returned, dims, preferred_element_type=jnp.float32
    )
    return (after_float + moe_out).astype(jnp.bfloat16)


def solution(mesh):
    placed = (
        P(("sp", "tp"), None),
        P("sp", "tp"),
        P("sp", "tp"),
        P("sp", "tp"),
        P("sp", "tp"),
        P("sp", "tp"),
        P("tp"),
        P(),
        P(),
        P(),
        P(("sp", "tp"), None),
        P(("sp", "tp"), None),
        P("sp", None, "tp"),
        P("sp", None, "tp"),
        P("sp", "tp", None),
    )
    return jax.shard_map(
        on_device, mesh=mesh, in_specs=placed, out_specs=P(("sp", "tp"), None), check_vma=False
    )
```

time: 652 us -> 213 us (0.33)
  blocking collectives: 290 us -> 0 us
  waiting for transfers between devices: 255 us -> 0 us
  Pallas kernels: 0 us -> 167 us
  local copies, waits for them, and re-layouts: 60.1 us -> 19.5 us
  matrix products: 10.1 us -> 24.4 us
  between operations: 13.8 us -> 0.47 us
  other arithmetic: 8.8 us -> 0.7 us
  starting transfers between devices: 6.53 us -> 0 us
    all_to_all x3 -> x0, blocking collectives: 290 us -> none  [the longest x1 279 us: on_device(): lax.all_to_all(doubled, ('sp', 'tp'), split_axis=0, concat_axis=0, tiled=...]
    all_gather x1 -> x0, waiting for transfers between devices: 226 us -> none  [sent_together(): lax.all_gather(both, axis, axis=dim, tiled=True)]
    pallas_call x0 -> x3, Pallas kernels: none -> 167 us  [the longest x1 99.5 us: attention(): pl.pallas_call(attention_kernel, out_shape=(jax.ShapeDtypeStruct((8, 128,...]
    all_to_all x1 -> x0, waiting for transfers between devices: 29.6 us -> none  [on_device(): lax.all_to_all(summed, 'sp', split_axis=0, concat_axis=0, tiled=True)]
    split x2 -> x0, local copies, waits for them, and re-layouts: 19.8 us -> none  [sent_together(): jnp.split(lax.all_gather(both, axis, axis=dim, tiled=True), ends, axis=al...]
    dot_general x8 -> x9, matrix products: 10.1 us -> 24.4 us  [the longest x1 5.31 us: on_device(): jnp.dot(other, down_other[0], preferred_element_type=jnp.float32)]
    unnamed x37 -> x48, local copies, waits for them, and re-layouts: 12.6 us -> 3.8 us
    gather x3 -> x0, local copies, waits for them, and re-layouts: 7.97 us -> none  [the longest x2 5.62 us: on_device(): routed[jnp.maximum(slot_rows, 0)]]
  transfers between devices with their start and end apart: 2 -> 0, of which waited for: 2 -> 0; matrix products, arithmetic and copies ran while one was open for 1% -> 0% of each run, Pallas kernels for 0% -> 0%
where the time goes in v1:
time: 213 us
  Pallas kernels  167 us (78%)
  matrix products  24.4 us (11%)
  local copies, waits for them, and re-layouts  19.5 us (9%)
    pallas_call x1, Pallas kernels, attention(): pl.pallas_call(attention_kernel, out_shape=(jax.ShapeDtypeStruct((8, 128,...  99.5 us
    pallas_call x2, Pallas kernels, exchange(): pl.pallas_call(exchange_kernel, out_shape=jax.ShapeDtypeStruct(x.shape, x...  68 us
    dot_general x1, matrix products, on_device(): jnp.dot(other, down_other[0], preferred_element_type=jnp.float32)  5.31 us
    dot_general x1, matrix products, on_device(): jnp.dot(own, down_weight[0], preferred_element_type=jnp.float32)  4.98 us

profile of v1, /device:TPU:2, one launch (start us, length us, event | category | flops | bytes accessed | tf_op | source)
XLA Modules:
  0.0 212.6 jit_solution(3451727037813218373)
XLA Ops:
  0.0 0.8 slice_bitcast_fusion.3
  0.8 0.1 fusion.37
  1.0 0.5 copy-done.16
  1.6 1.0 copy.19
  2.6 0.2 copy.21
  2.8 0.0 copy-done.14
  2.8 0.1 copy.20
  2.9 0.0 copy-start.15
  2.9 0.2 copy.22
  3.1 0.1 maximum_bitcast_fusion
  3.2 0.0 copy-done.13
  3.2 0.1 reshape.241
  3.3 0.2 copy.23
  3.5 0.0 copy-start.20
  3.5 0.0 copy-start.21
  3.5 0.0 copy-start
  3.5 0.0 copy-start.1
  3.6 0.2 copy-done.15
  3.8 0.1 copy.24
  3.9 1.2 copy.25
  5.2 0.0 copy-start.6
  5.2 0.4 fusion.30
  5.6 0.0 copy-done.20
  5.6 0.1 broadcast_in_dim.56.gain_in
  5.7 0.0 copy-done.21
  5.7 0.1 broadcast_in_dim.55.lam_in
  5.8 0.0 copy-done
  5.8 0.0 copy-done.1
  5.8 0.6 copy-done.6
  6.4 99.5 %shard_map.145 = (bf16[8,128,128]{2,1,0:T(8,128)(2,1)S(1)}, bf16[1,2048,256]{2,1,0:T(8,128)(2,1)S(1)}, bf16[1,2048,256]{2,1,0:T(8,128)(2,1)S(1)}, bf16[1,256,2048]{2,1,0:T(8,128)(2,1)S(1)}) custom-call(bf16[4,512,128]{2,1,0:T(8,128)(2,1)S(1)} %pad_maximum_fusion.kv_in, bf16[4,256,128]{2,1,0:T(8,128)(2,1)S(1)} %bitcast.53, ...), custom_call_target="tpu_custom_call" | custom-call | tf_op jit(solution)/shard_map/pallas_call | solution.py:248
  105.9 0.0 copy-start.2
  106.0 0.0 copy-start.4
  106.0 0.0 copy-start.8
  106.0 0.0 copy-done.12
  106.0 0.0 copy-start.18
  106.0 4.1 %multiply_reduce_fusion = (f32[128]{0:T(128)S(1)}, f32[128,2048]{1,0:T(8,128)S(1)}) fusion(bf16[1024,128]{1,0:T(8,128)(2,1)S(1)} %bitcast.54, bf16[1024,2048]{1,0:T(8,128)(2,1)} %param.23, bf16[128,2048]{1,0:T(8,128)(2,1)S(1)} %copy-done.12), kind=kOutput, calls=%fused_computation.22 | convolution fusion | flops 538443648 | bytes 6029824 | tf_op jit(solution)/shard_map/dot_general | solution.py:359
  110.1 0.0 copy-done.2
  110.1 0.0 copy-done.4
  110.1 0.0 copy-done.8
  110.2 0.0 copy-start.10
  110.2 0.1 eq.96
  110.3 0.0 copy-done.18
  110.3 1.8 convolution_convert_fusion
  112.1 3.8 %reshape.245.x = bf16[64,3,2,2048]{3,2,1,0:T(2,128)(2,1)} reshape(bf16[384,2048]{1,0:T(8,128)(2,1)} %convolution_convert_fusion) | data formatting | bytes 3145728 | tf_op jit(solution)/shard_map/reshape | solution.py:388
  115.9 0.0 copy-done.10
  115.9 35.1 %exchange1.1 = bf16[64,3,2,2048]{3,2,1,0:T(2,128)(2,1)} custom-call(bf16[64,3,2,2048]{3,2,1,0:T(2,128)(2,1)} %reshape.245.x), custom_call_target="tpu_custom_call" | custom-call | tf_op jit(solution)/shard_map/exchange1/pallas_call | solution.py:318
  151.0 0.0 copy-start.7
  151.0 3.7 %reshape.246 = bf16[384,2048]{1,0:T(8,128)(2,1)} reshape(bf16[64,3,2,2048]{3,2,1,0:T(2,128)(2,1)} %exchange1.1) | data formatting | bytes 3145728 | tf_op jit(solution)/shard_map/reshape | solution.py:388
  154.7 2.0 fusion.15
  156.7 0.0 copy-start.9
  156.7 5.0 %fusion.6 = f32[384,2048]{1,0:T(8,128)} fusion(bf16[384,2048]{1,0:T(8,128)(2,1)} %reshape.246, bf16[1,256,2048]{2,1,0:T(8,128)(2,1)S(1)} %copy-done.1, bf16[1,2048,256]{2,1,0:T(8,128)(2,1)S(1)} %copy-done, f32[384,256]{1,0:T(8,128)S(1)} %fusion.15), kind=kOutput, calls=%fused_computation.12 | convolution fusion | flops 805896192 | bytes 7208960 | tf_op jit(solution)/shard_map/dot_general | solution.py:391
  161.7 2.1 %fusion.10 = f32[384,256]{1,0:T(8,128)S(1)} fusion(bf16[384,2048]{1,0:T(8,128)(2,1)} %reshape.246, bf16[1,2048,256]{2,1,0:T(8,128)(2,1)S(1)} %copy-done.9), kind=kOutput, calls=%fused_computation.15 | convolution fusion | flops 402653184 | bytes 3014656 | tf_op jit(solution)/shard_map/dot_general | solution.py:332
  163.8 0.0 copy-done.3
  163.9 0.0 copy-done.5
  163.9 5.3 %add_convert_fusion = bf16[384,2048]{1,0:T(8,128)(2,1)} fusion(f32[384,2048]{1,0:T(8,128)} %fusion.6, bf16[384,2048]{1,0:T(8,128)(2,1)} %reshape.246, bf16[1,256,2048]{2,1,0:T(8,128)(2,1)S(1)} %copy-done.5, bf16[1,2048,256]{2,1,0:T(8,128)(2,1)S(1)} %copy-done.3, f32[384,256]{1,0:T(8,128)S(1)} %fusion.10), kind=kOutput, calls=%fused_computation | convolution fusion | flops 807469056 | bytes 8781824 | tf_op jit(solution)/shard_map/dot_general | solution.py:391
  169.2 3.7 %reshape.247.x = bf16[64,3,2,2048]{3,2,1,0:T(2,128)(2,1)} reshape(bf16[384,2048]{1,0:T(8,128)(2,1)} %add_convert_fusion) | data formatting | bytes 3145728 | tf_op jit(solution)/shard_map/reshape | solution.py:394
  172.9 32.9 %exchange2.1 = bf16[64,3,2,2048]{3,2,1,0:T(2,128)(2,1)} custom-call(bf16[64,3,2,2048]{3,2,1,0:T(2,128)(2,1)} %reshape.247.x), custom_call_target="tpu_custom_call" | custom-call | tf_op jit(solution)/shard_map/exchange2/pallas_call | solution.py:318
  205.8 0.0 copy-start.19
  205.8 0.0 copy-start.17
  205.8 2.5 %reshape.248 = bf16[384,2048]{1,0:T(8,128)(2,1)S(1)} reshape(bf16[64,3,2,2048]{3,2,1,0:T(2,128)(2,1)} %exchange2.1) | data formatting | bytes 3145728 | tf_op jit(solution)/shard_map/reshape | solution.py:395
  208.4 0.0 copy-done.19
  208.4 0.1 fusion.29
  208.6 1.4 fusion.46
  210.1 2.5 %fusion.1 = bf16[128,2048]{1,0:T(8,128)(2,1)} fusion(f32[128,2048]{1,0:T(8,128)S(1)} %copy-done.11, f32[128,2048]{1,0:T(8,128)} %fusion.46, bf16[384,128]{1,0:T(8,128)(2,1)S(1)} %convert_element_type.72, bf16[384,2048]{1,0:T(8,128)(2,1)S(1)} %reshape.248), kind=kOutput, calls=%fused_computation.5 | convolution fusion | flops 202113024 | bytes 4292608 | tf_op jit(solution)/shard_map/dot_general | solution.py:399
  (26 shorter events, 0.4 us)
Async XLA Ops:
  0.0 2.8 %copy-start.14 = (bf16[256,256]{1,0:T(8,128)(2,1)S(1)}, bf16[256,256]{1,0:T(8,128)(2,1)}, u32[]{:S(2)}) copy-start(bf16[256,256]{1,0:T(8,128)(2,1)} %param.19) | copy-start | bytes 393220
  0.0 3.2 %copy-start.13 = (bf16[256,512]{1,0:T(8,128)(2,1)S(1)}, bf16[256,512]{1,0:T(8,128)(2,1)}, u32[]{:S(2)}) copy-start(bf16[256,512]{1,0:T(8,128)(2,1)} %param.20) | copy-start | bytes 786436
  0.9 0.6 copy-start.16
  2.9 0.9 copy-start.15
  3.5 2.1 copy-start.20
  3.5 2.2 %copy-start.21 = (f32[4]{0:T(128)S(1)}, f32[4]{0:T(128)}, u32[]{:S(2)}) copy-start(f32[4]{0:T(128)} %param.21) | copy-start | bytes 52
  3.5 2.3 %copy-start = (bf16[1,2048,256]{2,1,0:T(8,128)(2,1)S(1)}, bf16[1,2048,256]{2,1,0:T(8,128)(2,1)}, u32[]{:S(2)}) copy-start(bf16[1,2048,256]{2,1,0:T(8,128)(2,1)} %up_in.1) | copy-start | bytes 3145732
  3.5 2.2 %copy-start.1 = (bf16[1,256,2048]{2,1,0:T(8,128)(2,1)S(1)}, bf16[1,256,2048]{2,1,0:T(8,128)(2,1)}, u32[]{:S(2)}) copy-start(bf16[1,256,2048]{2,1,0:T(8,128)(2,1)} %down_in.1) | copy-start | bytes 3145732
  5.2 1.2 copy-start.6
  6.4 99.6 %copy-start.12 = (bf16[128,2048]{1,0:T(8,128)(2,1)S(1)}, bf16[128,2048]{1,0:T(8,128)(2,1)}, u32[]{:S(2)}) copy-start(bf16[128,2048]{1,0:T(8,128)(2,1)} %param.15) | copy-start | bytes 1572868
  105.9 4.2 %copy-start.2 = (bf16[1,2048,256]{2,1,0:T(8,128)(2,1)}, bf16[1,2048,256]{2,1,0:T(8,128)(2,1)S(1)}, u32[]{:S(2)}) copy-start(bf16[1,2048,256]{2,1,0:T(8,128)(2,1)S(1)} %get-tuple-element.11) | copy-start | bytes 3145732
  106.0 4.2 %copy-start.4 = (bf16[1,256,2048]{2,1,0:T(8,128)(2,1)}, bf16[1,256,2048]{2,1,0:T(8,128)(2,1)S(1)}, u32[]{:S(2)}) copy-start(bf16[1,256,2048]{2,1,0:T(8,128)(2,1)S(1)} %get-tuple-element.12) | copy-start | bytes 3145732
  106.0 4.2 %copy-start.8 = (bf16[1,2048,256]{2,1,0:T(8,128)(2,1)}, bf16[1,2048,256]{2,1,0:T(8,128)(2,1)S(1)}, u32[]{:S(2)}) copy-start(bf16[1,2048,256]{2,1,0:T(8,128)(2,1)S(1)} %get-tuple-element.10) | copy-start | bytes 3145732
  106.0 4.3 %copy-start.18 = (f32[2048]{0:T(1024)S(1)}, f32[2048]{0:T(1024)}, u32[]{:S(2)}) copy-start(f32[2048]{0:T(1024)} %param.24) | copy-start | bytes 24580
  110.2 5.7 %copy-start.10 = (f32[128,2048]{1,0:T(8,128)}, f32[128,2048]{1,0:T(8,128)S(1)}, u32[]{:S(2)}) copy-start(f32[128,2048]{1,0:T(8,128)S(1)} %get-tuple-element.20) | copy-start | bytes 3145732
  151.0 3.7 %copy-start.7 = (bf16[1,2048,256]{2,1,0:T(8,128)(2,1)S(1)}, bf16[1,2048,256]{2,1,0:T(8,128)(2,1)}, u32[]{:S(2)}) copy-start(bf16[1,2048,256]{2,1,0:T(8,128)(2,1)} %gate_in.1) | copy-start | bytes 3145732
  156.7 5.0 %copy-start.9 = (bf16[1,2048,256]{2,1,0:T(8,128)(2,1)S(1)}, bf16[1,2048,256]{2,1,0:T(8,128)(2,1)}, u32[]{:S(2)}) copy-start(bf16[1,2048,256]{2,1,0:T(8,128)(2,1)} %copy-done.8) | copy-start | bytes 3145732
  161.7 2.1 %copy-start.3 = (bf16[1,2048,256]{2,1,0:T(8,128)(2,1)S(1)}, bf16[1,2048,256]{2,1,0:T(8,128)(2,1)}, u32[]{:S(2)}) copy-start(bf16[1,2048,256]{2,1,0:T(8,128)(2,1)} %copy-done.2) | copy-start | bytes 3145732
  161.7 2.2 %copy-start.5 = (bf16[1,256,2048]{2,1,0:T(8,128)(2,1)S(1)}, bf16[1,256,2048]{2,1,0:T(8,128)(2,1)}, u32[]{:S(2)}) copy-start(bf16[1,256,2048]{2,1,0:T(8,128)(2,1)} %copy-done.4) | copy-start | bytes 3145732
  205.8 2.5 %copy-start.19 = (f32[128,2]{0,1:T(2,128)S(1)}, f32[128,2]{0,1:T(2,128)}, u32[]{:S(2)}) copy-start(f32[128,2]{0,1:T(2,128)} %param.26) | copy-start | bytes 3076
  205.8 2.6 %copy-start.17 = (f32[64,128]{1,0:T(8,128)S(1)}, f32[64,128]{1,0:T(8,128)}, u32[]{:S(2)}) copy-start(f32[64,128]{1,0:T(8,128)} %copy-done.16) | copy-start | bytes 98308
  208.5 1.5 copy-start.11

commit v2 on v0

v2 whole, which is shorter than its diff:
```python
import jax
import jax.numpy as jnp
from jax import lax
from jax.experimental import pallas as pl
from jax.experimental.pallas import tpu as pltpu
from jax.sharding import PartitionSpec as P

epsilon = 1e-06
low_value = -1e30
MESH = pl.DeviceIdType.MESH
CAP = 6
WIDTH = 2048
SINGLES = (1, 2, 4)
DOUBLES = (3, 5, 6)
ORDERS = ((1, 2, 4), (2, 4, 1), (4, 1, 2), (1, 2, 4))
f32 = jnp.float32
bf16 = jnp.bfloat16


def to_class(p):
    return ((p + 1) // 2) % 2, p // 2


def to_coord(a, g):
    return 2 * g + (a + g) % 2


def sp_of(a, g):
    return to_coord(a[0], g[0]) * 16 + to_coord(a[1], g[1]) * 4 + to_coord(a[2], g[2])


def flipped(a, mask):
    return ((a[0] + mask // 4) % 2, (a[1] + (mask // 2) % 2) % 2, (a[2] + mask % 2) % 2)


class Place:
    def __init__(self):
        self.sp = lax.axis_index("sp")
        self.tp = lax.axis_index("tp")
        coords = (self.sp // 16, (self.sp // 4) % 4, self.sp % 4)
        pairs = [to_class(p) for p in coords]
        self.z = coords[0]
        self.a = tuple(p[0] for p in pairs)
        self.g = tuple(p[1] for p in pairs)
        self.parity = (self.g[0] + self.g[1] + self.g[2]) % 2
        self.head = self.g[0] * 4 + self.g[1] * 2 + self.g[2]

    def source_g(self, j, core):
        gz, gy = j // 2, j % 2
        return (gz, gy, (core + gz + gy) % 2)


def remote(src, dst, send, recv, device):
    return pltpu.make_async_remote_copy(
        src_ref=src, dst_ref=dst, send_sem=send, recv_sem=recv, device_id=device, device_id_type=MESH
    )


def arrival(at, sem):
    pltpu.make_async_copy(at, at, sem).wait()


def iota(shape, dim):
    return lax.broadcasted_iota(jnp.int32, shape, dim)


def layer_kernel(
    q1_in, k1_in, q2_in, k2_in, v_in, lam_in, gain_in, res_in, ng_in, ids_in, rw_in,
    ow_in, gate_in, up_in, down_in,
    out_ref,
    kv_own, q_own, lam_own, kv_all, q_all, lam_all, q_wide, acc, m_ref, l_ref, att_send, att_recv,
    ow, gate, up, down, after, routed, pick, blend, perm, perm_back, out_buf, arr_buf, ret_buf, got_buf,
    s1_send, s1_recv, s2_send, s2_recv, sib_send, sib_recv, att_ssem, att_rsem,
    w_local, w_send, w_recv, d_send, d_recv, r_send, r_recv,
):
    me = Place()
    sibling = (me.sp, 1 - me.tp)
    barrier = pltpu.get_barrier_semaphore()

    @pl.loop(1, 64)
    def _(i):
        pl.semaphore_signal(barrier, inc=1, device_id=((me.sp + i) % 64, me.tp), device_id_type=MESH)

    for g in range(8):
        chip = sp_of(me.a, (g // 4, (g // 2) % 2, g % 2))
        pl.semaphore_signal(barrier, inc=1, device_id=(chip, 1 - me.tp), device_id_type=MESH)

    own_copies = [
        pltpu.make_async_copy(gate_in.at[0], gate.at[0], w_local.at[0]),
        pltpu.make_async_copy(up_in.at[0], up.at[0], w_local.at[1]),
        pltpu.make_async_copy(down_in.at[0], down.at[0], w_local.at[2]),
        pltpu.make_async_copy(ow_in, ow, w_local.at[3]),
    ]
    for c in own_copies:
        c.start()

    lane = iota((256, 128), 1)
    for pair in range(2):
        at = pl.ds(pair * 128, 128)
        k1, k2 = k1_in[:, at].astype(f32), k2_in[:, at].astype(f32)
        q1, q2 = q1_in[:, at].astype(f32) * 0.125, q2_in[:, at].astype(f32) * 0.125
        for odd in range(2):
            hl = pair * 2 + odd
            if odd:
                keys = jnp.where(lane < 64, pltpu.roll(k1, 64, 1), k2)
                queries = jnp.where(lane < 64, pltpu.roll(q1, 64, 1), q2)
            else:
                keys = jnp.where(lane < 64, k1, pltpu.roll(k2, 64, 1))
                queries = jnp.where(lane < 64, q1, pltpu.roll(q2, 64, 1))
            kv_own[hl, 0:256, :] = keys.astype(bf16)
            for b in range(2):
                rows = slice(b * 128, b * 128 + 128)
                value = v_in[rows, hl * 128 : hl * 128 + 128].astype(f32)
                kv_own[hl, 256 + b * 128 : 384 + b * 128, :] = value.T.astype(bf16)
                q_own[hl, rows, :] = queries[rows, :].T.astype(bf16)
            lam_own[hl] = jnp.full((8, 128), lam_in[hl], f32)
    pl.semaphore_wait(barrier, 71)

    j_me = me.g[0] * 2 + me.g[1]
    for hl in range(4):
        chip = sp_of(me.a, (me.tp, hl // 2, hl % 2))
        itself = (chip == me.sp) & (me.parity == me.tp)
        parts = (
            (kv_own.at[hl], kv_all.at[me.sp]),
            (q_own.at[hl], q_all.at[j_me]),
            (lam_own.at[hl], lam_all.at[j_me]),
        )

        @pl.when(itself)
        def _():
            for n, (src, dst) in enumerate(parts):
                pltpu.make_async_copy(src, dst, s1_recv.at[n, j_me]).start()

        @pl.when(jnp.logical_not(itself))
        def _():
            for n, (src, dst) in enumerate(parts):
                remote(src, dst, s1_send.at[n, hl], s1_recv.at[n, j_me], (chip, me.parity)).start()

    ids0, ids1 = ids_in[0:1, :], ids_in[1:2, :]
    rw0, rw1 = rw_in[0:1, :], rw_in[1:2, :]
    upper = jnp.where(iota((128, 128), 0) < iota((128, 128), 1), 1.0, 0.0).astype(bf16)
    small = iota((128, 128), 0)
    for blk in range(4):
        expert = blk * 16 + (small % 32) // 2
        place = (small // 32) * 2 + small % 2
        hit0, hit1 = ids0 == expert, ids1 == expert
        hit = jnp.where(hit0 | hit1, 1.0, 0.0)
        rank = jnp.dot(hit.astype(bf16), upper, preferred_element_type=f32)
        chosen = jnp.where(rank == place.astype(f32), hit, 0.0)
        pick[blk * 128 : blk * 128 + 128, :] = chosen.astype(bf16)
        share = chosen * (jnp.where(hit0, rw0, 0.0) + jnp.where(hit1, rw1, 0.0))
        share = share.T
        high = share.astype(bf16)
        blend[0:128, blk * 128 : blk * 128 + 128] = high
        blend[128:256, blk * 128 : blk * 128 + 128] = (share - high.astype(f32)).astype(bf16)
    ia, ib = iota((256, 256), 0), iota((256, 256), 1)
    packed_a = ((ia // 2) % 16) * 16 + (ia % 2) * 8 + ia // 32
    packed_b = ((ib // 2) % 16) * 16 + (ib % 2) * 8 + ib // 32
    perm[...] = jnp.where(packed_a == ib, 1.0, 0.0).astype(bf16)
    perm_back[...] = jnp.where(packed_b == ia, 1.0, 0.0).astype(bf16)

    w_copies = [
        remote(src.at[0], dst.at[1], w_send.at[n], w_recv.at[n], sibling)
        for n, (src, dst) in enumerate(((gate_in, gate), (up_in, up), (down_in, down)))
    ]

    def tile_at(j, rel, core):
        return sp_of(flipped(me.a, rel), me.source_g(j, core))

    def hop(j, rel, bit):
        target = (sp_of(flipped(me.a, bit), me.g), me.tp)
        at = kv_all.at[tile_at(j, rel, me.tp)]
        return remote(at, at, s2_send.at[j, rel ^ bit], s2_recv.at[j, rel ^ bit], target)

    def across(j, rel):
        at = kv_all.at[tile_at(j, rel, me.tp)]
        return remote(at, at, sib_send.at[j, rel], sib_recv.at[j, rel], sibling)

    for j in range(4):
        arrival(kv_all.at[tile_at(j, 0, me.tp)], s1_recv.at[0, j])
        for bit in ORDERS[j]:
            hop(j, 0, bit).start()
        across(j, 0).start()
    for c in w_copies:
        c.start()

    for j in range(4):
        arrival(q_all.at[j], s1_recv.at[1, j])
        arrival(lam_all.at[j], s1_recv.at[2, j])


    def diagonal(j, carry):
        full = jnp.concatenate([q_all[j, 0:128, :], q_all[j, 128:256, :]], axis=1)
        row = iota((128, 256), 0)
        zero = jnp.zeros_like(full)
        q_wide[j, :, 0:256] = jnp.where(row < 64, full, zero)
        q_wide[j, :, 256:512] = jnp.where(row >= 64, full, zero)
        t = tile_at(j, 0, me.tp)
        s = jnp.dot(kv_all[t, 0:256, :], q_wide[j], preferred_element_type=f32)
        s = jnp.where(iota(s.shape, 0) <= iota(s.shape, 1) % 256, s, low_value)
        m = jnp.max(s, axis=0, keepdims=True)
        p = jnp.exp(s - m)
        m_ref[j] = m
        l_ref[j] = jnp.sum(p, axis=0, keepdims=True)
        values = jnp.concatenate([kv_all[t, 256:384, :], kv_all[t, 384:512, :]], axis=1)
        acc[j] = jnp.dot(values, p.astype(bf16), preferred_element_type=f32)
        return carry

    lax.fori_loop(0, 4, diagonal, 0)

    def scores(t, j):
        return jnp.dot(kv_all[t, 0:256, :], q_wide[j], preferred_element_type=f32)

    def tiles_step(tiles, j):
        m, l = m_ref[j], l_ref[j]
        s = scores(tiles[0], j)
        for i, t in enumerate(tiles):
            following = scores(tiles[i + 1], j) if i + 1 < len(tiles) else None
            newest = jnp.maximum(m, jnp.max(s, axis=0, keepdims=True))
            p = jnp.exp(s - newest)
            factor = jnp.exp(m - newest)
            l = l * factor + jnp.sum(p, axis=0, keepdims=True)
            values = jnp.concatenate([kv_all[t, 256:384, :], kv_all[t, 384:512, :]], axis=1)
            acc[j] = acc[j] * factor + jnp.dot(values, p.astype(bf16), preferred_element_type=f32)
            m, s = newest, following
        m_ref[j] = m
        l_ref[j] = l

    def received(rels, gz):
        for j in (2 * gz, 2 * gz + 1):
            order = ORDERS[j]
            for rel in rels:
                arrival(kv_all.at[tile_at(j, rel, me.tp)], s2_recv.at[j, rel])
                last = max(order.index(b) for b in order if rel & b)
                for b in order[last + 1 :]:
                    hop(j, rel, b).start()
                across(j, rel).start()

    groups = ((2, SINGLES, 0), (5, SINGLES, 1), (8, DOUBLES, 0), (11, DOUBLES, 1), (14, (7,), 0), (15, (7,), 1))

    def unit(n, carry):
        for start, rels, gz_static in groups:

            @pl.when(n == start)
            def _():
                received(rels, gz_static)

        third = (n + 1) % 3
        gz = jnp.where(n < 2, n, jnp.where(n < 14, ((n - 2) // 3) % 2, n - 14))
        single = jnp.where(third == 0, 1, jnp.where(third == 1, 2, 4))
        double = jnp.where(third == 0, 3, jnp.where(third == 1, 5, 6))
        rel = jnp.where(n < 2, 0, jnp.where(n < 8, single, jnp.where(n < 14, double, 7)))
        for half in range(2):
            j = 2 * gz + half
            arrival(kv_all.at[tile_at(j, rel, 1 - me.tp)], sib_recv.at[j, rel])
        a_there = flipped(me.a, rel)
        tiles = [sp_of(a_there, (gz, y, x)) for y in range(2) for x in range(2)]
        far = rel // 4 == 1

        def one_query(j, inner):
            gz_q = j // 2
            same = gz_q == gz
            s_own = tile_at(j, 0, me.tp)
            whole = (gz < gz_q) | (same & far & ((me.a[0] + gz) % 2 == 1))

            @pl.when(whole)
            def _():
                tiles_step(tiles, j)

            @pl.when(same & jnp.logical_not(far))
            def _():
                def one(i, c):
                    t = sp_of(a_there, (gz, i // 2, i % 2))

                    @pl.when(t < s_own)
                    def _():
                        tiles_step([t], j)

                    return c

                lax.fori_loop(0, 4, one, 0)

            return inner

        return lax.fori_loop(0, 4, one_query, carry)

    lax.fori_loop(0, 16, unit, 0)

    def finish(j, carry):
        total = acc[j] / l_ref[j]
        for b in range(2):
            first = total[:, 128 * b : 128 * b + 128]
            second = total[:, 256 + 128 * b : 384 + 128 * b]
            out = first - lam_all[0, 0:1, :] * second
            mean = jnp.mean(out * out, axis=0, keepdims=True)
            out = (out * lax.rsqrt(mean + epsilon)).T * gain_in[...]
            att_send[j, b] = out.astype(bf16)
        chip = tile_at(j, 0, me.tp)
        for b in range(2):
            itself = (chip == me.sp) & (me.tp == b)

            @pl.when(itself)
            def _():
                pltpu.make_async_copy(att_send.at[j, b], att_recv.at[me.head], att_rsem.at[me.head]).start()

            @pl.when(jnp.logical_not(itself))
            def _():
                remote(
                    att_send.at[j, b], att_recv.at[me.head], att_ssem.at[j, b], att_rsem.at[me.head], (chip, b)
                ).start()

        return carry

    lax.fori_loop(0, 4, finish, 0)

    own_copies[3].wait()
    for h in range(8):
        arrival(att_recv.at[h], att_rsem.at[h])
    attended = jnp.concatenate([att_recv[h] for h in range(8)], axis=1)

    def project(n, square):
        at = pl.ds(pl.multiple_of(n * 512, 512), 512)
        value = res_in[:, at].astype(f32) + jnp.dot(attended, ow[:, at], preferred_element_type=f32)
        value = value.astype(bf16)
        after[:, at] = value
        value = value.astype(f32)
        return square + jnp.sum(value * value, axis=1, keepdims=True)

    square = lax.fori_loop(0, 4, project, jnp.zeros((128, 1), f32))
    inverse = lax.rsqrt(square * (1.0 / WIDTH) + epsilon)

    def norm(n, carry):
        at = pl.ds(pl.multiple_of(n * 512, 512), 512)
        routed[:, at] = (after[:, at].astype(f32) * inverse * ng_in[:, at]).astype(bf16)
        return carry

    lax.fori_loop(0, 4, norm, 0)

    def packed(value, into, blk):
        rows = pl.ds(pl.multiple_of(blk * 256, 256), 256)
        for c in range(3):
            stacked = jnp.concatenate(
                [value[c * 32 : c * 32 + 32, k * 256 : k * 256 + 256] for k in range(8)], axis=0
            )
            block = jnp.dot(perm_back[...], stacked, preferred_element_type=f32).astype(bf16)
            into[pl.ds(blk * 16, 16), :, c * 256 : c * 256 + 256] = block.reshape(16, 16, 256)

    def unpacked(source, blk, extra):
        parts = []
        for c in range(3):
            block = source[pl.ds(blk * 16, 16), :, c * 256 : c * 256 + 256].reshape(256, 256)
            parts.append(jnp.dot(perm[...], block, preferred_element_type=f32).astype(bf16))
        columns = []
        for k in range(8):
            pieces = [part[k * 32 : k * 32 + 32, :] for part in parts]
            if extra:
                pieces.append(jnp.zeros((32, 256), bf16))
            columns.append(jnp.concatenate(pieces, axis=0))
        return jnp.concatenate(columns, axis=1)

    def block_of(step):
        shift = jnp.where(step == 2, 3, jnp.where(step == 3, 2, step))
        return (me.z + shift) % 4

    def spread(blk, source, target, ssem, rsem):
        def one(i, carry):
            to = blk * 16 + (me.sp + 15 - i) % 16

            @pl.when(to == me.sp)
            def _():
                pltpu.make_async_copy(source.at[to], target.at[me.sp], rsem.at[me.sp]).start()

            @pl.when(to != me.sp)
            def _():
                remote(source.at[to], target.at[me.sp], ssem.at[to], rsem.at[me.sp], (to, me.tp)).start()

            return carry

        lax.fori_loop(0, 16, one, 0)

    def collect(blk, target, rsem):
        def one(i, carry):
            arrival(target.at[blk * 16 + i], rsem.at[blk * 16 + i])
            return carry

        lax.fori_loop(0, 16, one, 0)

    def dispatch(step, carry):
        blk = block_of(step)
        rows = pl.ds(pl.multiple_of(blk * 128, 128), 128)
        value = jnp.dot(pick[rows, :], routed[...], preferred_element_type=f32).astype(bf16)
        packed(value, out_buf, blk)
        spread(blk, out_buf, arr_buf, d_send, d_recv)
        return carry

    lax.fori_loop(0, 4, dispatch, 0)

    for c in own_copies[:3]:
        c.wait()
    for c in w_copies:
        c.wait()

    def work(step, carry):
        blk = block_of(step)
        collect(blk, arr_buf, d_recv)
        x = unpacked(arr_buf, blk, False)
        hidden = []
        for half in range(2):
            g = jnp.dot(x, gate[half], preferred_element_type=f32)
            u = jnp.dot(x, up[half], preferred_element_type=f32)
            hidden.append((g * jax.nn.sigmoid(g) * u).astype(bf16))
        y = jnp.dot(hidden[0], down[0], preferred_element_type=f32) + jnp.dot(
            hidden[1], down[1], preferred_element_type=f32
        )
        packed(y.astype(bf16), ret_buf, blk)
        spread(blk, ret_buf, got_buf, r_send, r_recv)
        return carry

    lax.fori_loop(0, 4, work, 0)

    made = []
    for blk in range(4):
        collect(blk, got_buf, r_recv)
        made.append(unpacked(got_buf, blk, True))
    for n in range(4):
        at = slice(n * 512, n * 512 + 512)
        column = jnp.concatenate([part[:, at] for part in made], axis=0)
        both = jnp.dot(blend[...], column, preferred_element_type=f32)
        out_ref[:, at] = (after[:, at].astype(f32) + (both[0:128] + both[128:256])).astype(bf16)

    for j in range(4):
        chip = tile_at(j, 0, me.tp)
        for b in range(2):

            @pl.when(jnp.logical_not((chip == me.sp) & (me.tp == b)))
            def _():
                arrival(att_send.at[j, b], att_ssem.at[j, b])

        for rel in range(8):
            if rel:
                arrival(kv_all.at[tile_at(j, 0, me.tp)], s2_send.at[j, rel])
            arrival(kv_all.at[tile_at(j, rel, me.tp)], sib_send.at[j, rel])
    for hl in range(4):
        chip = sp_of(me.a, (me.tp, hl // 2, hl % 2))

        @pl.when(jnp.logical_not((chip == me.sp) & (me.parity == me.tp)))
        def _():
            for n, src in enumerate((kv_own, q_own, lam_own)):
                arrival(src.at[hl], s1_send.at[n, hl])

    @pl.loop(0, 64)
    def _(i):
        @pl.when(i != me.sp)
        def _():
            arrival(out_buf.at[i], d_send.at[i])
            arrival(ret_buf.at[i], r_send.at[i])


def on_device(
    residual, query_one, key_one, query_two, key_two, value_rows, lambda_head, head_gain, out_weight,
    norm_gain, route_ids, route_weights, gate_weight, up_weight, down_weight,
):
    vmem = pl.BlockSpec(memory_space=pltpu.VMEM)
    smem = pl.BlockSpec(memory_space=pltpu.SMEM)
    anywhere = pl.BlockSpec(memory_space=pl.ANY)
    dma = pltpu.SemaphoreType.DMA
    V = pltpu.VMEM
    return pl.pallas_call(
        layer_kernel,
        out_shape=jax.ShapeDtypeStruct(residual.shape, bf16),
        in_specs=[vmem] * 5 + [smem] + [vmem] * 5 + [anywhere] * 4,
        out_specs=vmem,
        scratch_shapes=[
            V((4, 512, 128), bf16), V((4, 256, 128), bf16), V((4, 8, 128), f32),
            V((64, 512, 128), bf16), V((4, 256, 128), bf16), V((4, 8, 128), f32),
            V((4, 128, 512), bf16), V((4, 128, 512), f32), V((4, 1, 512), f32), V((4, 1, 512), f32),
            V((4, 2, 128, 128), bf16), V((8, 128, 128), bf16),
            V((1024, WIDTH), bf16), V((2, WIDTH, 256), bf16), V((2, WIDTH, 256), bf16),
            V((2, 256, WIDTH), bf16), V((128, WIDTH), bf16), V((128, WIDTH), bf16),
            V((512, 128), bf16), V((256, 512), bf16), V((256, 256), bf16), V((256, 256), bf16),
            V((64, 16, 768), bf16), V((64, 16, 768), bf16), V((64, 16, 768), bf16), V((64, 16, 768), bf16),
            dma((3, 4)), dma((3, 4)), dma((4, 8)), dma((4, 8)), dma((4, 8)), dma((4, 8)),
            dma((4, 2)), dma((8,)), dma((4,)), dma((3,)), dma((3,)),
            dma((64,)), dma((64,)), dma((64,)), dma((64,)),
        ],
        compiler_params=pltpu.CompilerParams(
            collective_id=0, has_side_effects=True, vmem_limit_bytes=56 * 1024 * 1024
        ),
        name="layer",
    )(
        query_one, key_one, query_two, key_two, value_rows, lambda_head, head_gain[None, :], residual,
        norm_gain[None, :], route_ids.T, route_weights.T, out_weight, gate_weight, up_weight, down_weight,
    )


def solution(mesh):
    placed = (
        P(("sp", "tp"), None),
        P("sp", "tp"),
        P("sp", "tp"),
        P("sp", "tp"),
        P("sp", "tp"),
        P("sp", "tp"),
        P("tp"),
        P(),
        P(),
        P(),
        P(("sp", "tp"), None),
        P(("sp", "tp"), None),
        P("sp", None, "tp"),
        P("sp", None, "tp"),
        P("sp", "tp", None),
    )
    return jax.shard_map(
        on_device, mesh=mesh, in_specs=placed, out_specs=P(("sp", "tp"), None), check_vma=False
    )
```

time: 652 us -> 146 us (0.22)
  blocking collectives: 290 us -> 0 us
  waiting for transfers between devices: 255 us -> 0 us
  Pallas kernels: 0 us -> 144 us
  local copies, waits for them, and re-layouts: 60.1 us -> 1.88 us
  between operations: 13.8 us -> 0.01 us
  matrix products: 10.1 us -> 0 us
  other arithmetic: 8.8 us -> 0 us
  starting transfers between devices: 6.53 us -> 0 us
    all_to_all x3 -> x0, blocking collectives: 290 us -> none  [the longest x1 279 us: on_device(): lax.all_to_all(doubled, ('sp', 'tp'), split_axis=0, concat_axis=0, tiled=...]
    all_gather x1 -> x0, waiting for transfers between devices: 226 us -> none  [sent_together(): lax.all_gather(both, axis, axis=dim, tiled=True)]
    pallas_call x0 -> x1, Pallas kernels: none -> 144 us  [on_device(): pl.pallas_call(layer_kernel, out_shape=jax.ShapeDtypeStruct(residual.shap...]
    all_to_all x1 -> x0, waiting for transfers between devices: 29.6 us -> none  [on_device(): lax.all_to_all(summed, 'sp', split_axis=0, concat_axis=0, tiled=True)]
    split x2 -> x0, local copies, waits for them, and re-layouts: 19.8 us -> none  [sent_together(): jnp.split(lax.all_gather(both, axis, axis=dim, tiled=True), ends, axis=al...]
    unnamed x37 -> x1, local copies, waits for them, and re-layouts: 12.6 us -> 1.88 us
    dot_general x8 -> x0, matrix products: 10.1 us -> none  [the longest x1 3.03 us: expert_rows(): gate = jnp.dot(rows, gate_half, preferred_element_type=jnp.float32)]
    reshape x2 -> x0, local copies, waits for them, and re-layouts: 9.02 us -> none  [the longest x1 6.42 us: on_device(): arrived.reshape(sources * items, width_rows)]
  transfers between devices with their start and end apart: 2 -> 0, of which waited for: 2 -> 0; matrix products, arithmetic and copies ran while one was open for 1% -> 0% of each run, Pallas kernels for 0% -> 0%
where the time goes in v2:
time: 146 us
  Pallas kernels  144 us (99%)
  local copies, waits for them, and re-layouts  1.88 us (1%)
    pallas_call x1, Pallas kernels, on_device(): pl.pallas_call(layer_kernel, out_shape=jax.ShapeDtypeStruct(residual.shap...  144 us

profile of v2, /device:TPU:2, one launch (start us, length us, event | category | flops | bytes accessed | tf_op | source)
XLA Modules:
  0.0 146.0 jit_solution(13181379150179389857)
XLA Ops:
  0.0 144.1 %layer.1 = bf16[128,2048]{1,0:T(8,128)(2,1)} custom-call(bf16[256,256]{1,0:T(8,128)(2,1)} %q1_in.1, bf16[256,256]{1,0:T(8,128)(2,1)} %k1_in.1, bf16[256,256]{1,0:T(8,128)(2,1)} %q2_in.1, bf16[256,256]{1,0:T(8,128)(2,1)} %k2_in.1, bf16[256,512]{1,0:T(8,128)(2,1)} %v_in.1, f32[4]{0:T(128)} %lam_in.1, f32[1,128]{1,0:T(1,128)} %bitcast.7, ...), custom_call_target="tpu_custom_call" | custom-call | tf_op jit(solution)/shard_map/layer/pallas_call | solution.py:468
  144.2 1.9 %copy.17 = bf16[128,2048]{1,0:T(8,128)(2,1)} copy(bf16[128,2048]{1,0:T(8,128)(2,1)} %layer.1) | data formatting | bytes 1048576

commit v3 on v2

--- a/solution.py
+++ b/solution.py
@@ -11,8 +11,6 @@
 CAP = 6
 WIDTH = 2048
 SINGLES = (1, 2, 4)
-DOUBLES = (3, 5, 6)
-ORDERS = ((1, 2, 4), (2, 4, 1), (4, 1, 2), (1, 2, 4))
 f32 = jnp.float32
 bf16 = jnp.bfloat16
 
@@ -117,24 +115,33 @@
     pl.semaphore_wait(barrier, 71)
 
     j_me = me.g[0] * 2 + me.g[1]
-    for hl in range(4):
+
+    def first_target(hl):
         chip = sp_of(me.a, (me.tp, hl // 2, hl % 2))
-        itself = (chip == me.sp) & (me.parity == me.tp)
-        parts = (
-            (kv_own.at[hl], kv_all.at[me.sp]),
-            (q_own.at[hl], q_all.at[j_me]),
-            (lam_own.at[hl], lam_all.at[j_me]),
-        )
-
-        @pl.when(itself)
-        def _():
-            for n, (src, dst) in enumerate(parts):
-                pltpu.make_async_copy(src, dst, s1_recv.at[n, j_me]).start()
-
-        @pl.when(jnp.logical_not(itself))
-        def _():
-            for n, (src, dst) in enumerate(parts):
-                remote(src, dst, s1_send.at[n, hl], s1_recv.at[n, j_me], (chip, me.parity)).start()
+        return chip, (chip == me.sp) & (me.parity == me.tp)
+
+    def first_sends(kinds):
+        for i in range(4):
+            hl = ((me.g[0] + i // 2) % 2) * 2 + (me.g[1] + i % 2) % 2
+            chip, itself = first_target(hl)
+            every = (
+                (kv_own.at[hl], kv_all.at[me.sp]),
+                (q_own.at[hl], q_all.at[j_me]),
+                (lam_own.at[hl], lam_all.at[j_me]),
+            )
+
+            @pl.when(itself)
+            def _():
+                for n in kinds:
+                    pltpu.make_async_copy(*every[n], s1_recv.at[n, j_me]).start()
+
+            @pl.when(jnp.logical_not(itself))
+            def _():
+                for n in kinds:
+                    remote(*every[n], s1_send.at[n, hl], s1_recv.at[n, j_me], (chip, me.parity)).start()
+
+    first_sends((0,))
+    first_sends((1, 2))
 
     ids0, ids1 = ids_in[0:1, :], ids_in[1:2, :]
     rw0, rw1 = rw_in[0:1, :], rw_in[1:2, :]
@@ -170,19 +177,70 @@
     def hop(j, rel, bit):
         target = (sp_of(flipped(me.a, bit), me.g), me.tp)
         at = kv_all.at[tile_at(j, rel, me.tp)]
-        return remote(at, at, s2_send.at[j, rel ^ bit], s2_recv.at[j, rel ^ bit], target)
+        return remote(at, at, s2_send.at[j, rel + bit], s2_recv.at[j, rel + bit], target)
+
+    def source_at(i):
+        return ((me.g[1] + i // 2) % 2) * 2 + (me.g[2] + i % 2) % 2
+
+    def bits_of(j):
+        first = jnp.where(j == 3, me.tp, j)
+        turns = [(first + p) % 3 for p in range(3)]
+        return [(k * k + k + 2) // 2 for k in turns]
 
     def across(j, rel):
         at = kv_all.at[tile_at(j, rel, me.tp)]
         return remote(at, at, sib_send.at[j, rel], sib_recv.at[j, rel], sibling)
 
-    for j in range(4):
+    def drain_first():
+        for hl in range(4):
+            @pl.when(jnp.logical_not(first_target(hl)[1]))
+            def _():
+                for n, src in enumerate((kv_own, q_own, lam_own)):
+                    arrival(src.at[hl], s1_send.at[n, hl])
+
+    def drain_keys():
+        for j in range(4):
+            for rel in range(8):
+                if rel:
+                    arrival(kv_all.at[tile_at(j, 0, me.tp)], s2_send.at[j, rel])
+                arrival(kv_all.at[tile_at(j, rel, me.tp)], sib_send.at[j, rel])
+        drain_first()
+
+    def drain_heads():
+        for j in range(4):
+            chip = tile_at(j, 0, me.tp)
+            for b in range(2):
+
+                @pl.when(jnp.logical_not((chip == me.sp) & (me.tp == b)))
+                def _():
+                    arrival(att_send.at[j, b], att_ssem.at[j, b])
+
+    def drain_rows(buffer, sem):
+        @pl.loop(0, 64)
+        def _(i):
+            @pl.when(i != me.sp)
+            def _():
+                arrival(buffer.at[i], sem.at[i])
+
+    for i in range(4):
+        j = source_at(i)
         arrival(kv_all.at[tile_at(j, 0, me.tp)], s1_recv.at[0, j])
-        for bit in ORDERS[j]:
+        for bit in SINGLES:
             hop(j, 0, bit).start()
         across(j, 0).start()
     for c in w_copies:
         c.start()
+
+    def received(level, i):
+        j = source_at(i)
+        bits = bits_of(j)
+        sets = (((0,), (1,), (2,)), ((0, 1), (0, 2), (1, 2)), ((0, 1, 2),))[level]
+        for places in sets:
+            rel = sum(bits[p] for p in places)
+            arrival(kv_all.at[tile_at(j, rel, me.tp)], s2_recv.at[j, rel])
+            for p in range(places[-1] + 1, 3):
+                hop(j, rel, bits[p]).start()
+            across(j, rel).start()
 
     for j in range(4):
         arrival(q_all.at[j], s1_recv.at[1, j])
@@ -206,47 +264,47 @@
         acc[j] = jnp.dot(values, p.astype(bf16), preferred_element_type=f32)
         return carry
 
+    received(0, 0)
     lax.fori_loop(0, 4, diagonal, 0)
-
-    def scores(t, j):
-        return jnp.dot(kv_all[t, 0:256, :], q_wide[j], preferred_element_type=f32)
 
     def tiles_step(tiles, j):
         m, l = m_ref[j], l_ref[j]
-        s = scores(tiles[0], j)
-        for i, t in enumerate(tiles):
-            following = scores(tiles[i + 1], j) if i + 1 < len(tiles) else None
+        groups_here = [tiles[i : i + 2] for i in range(0, len(tiles), 2)]
+
+        def scores(group):
+            keys = jnp.concatenate([kv_all[t, 0:256, :] for t in group], axis=0)
+            return jnp.dot(keys, q_wide[j], preferred_element_type=f32)
+
+        s = scores(groups_here[0])
+        for i, group in enumerate(groups_here):
+            following = scores(groups_here[i + 1]) if i + 1 < len(groups_here) else None
             newest = jnp.maximum(m, jnp.max(s, axis=0, keepdims=True))
-            p = jnp.exp(s - newest)
+            p = jnp.exp(s - newest).astype(bf16)
             factor = jnp.exp(m - newest)
-            l = l * factor + jnp.sum(p, axis=0, keepdims=True)
-            values = jnp.concatenate([kv_all[t, 256:384, :], kv_all[t, 384:512, :]], axis=1)
-            acc[j] = acc[j] * factor + jnp.dot(values, p.astype(bf16), preferred_element_type=f32)
+            values = jnp.concatenate(
+                [kv_all[t, 256 + 128 * b : 384 + 128 * b, :] for t in group for b in range(2)], axis=1
+            )
+            values = jnp.concatenate([values, jnp.ones((16, values.shape[1]), bf16)], axis=0)
+            product = jnp.dot(values, p, preferred_element_type=f32)
+            l = l * factor + product[128:129]
+            acc[j] = acc[j] * factor + product[0:128]
             m, s = newest, following
         m_ref[j] = m
         l_ref[j] = l
 
-    def received(rels, gz):
-        for j in (2 * gz, 2 * gz + 1):
-            order = ORDERS[j]
-            for rel in rels:
-                arrival(kv_all.at[tile_at(j, rel, me.tp)], s2_recv.at[j, rel])
-                last = max(order.index(b) for b in order if rel & b)
-                for b in order[last + 1 :]:
-                    hop(j, rel, b).start()
-                across(j, rel).start()
-
-    groups = ((2, SINGLES, 0), (5, SINGLES, 1), (8, DOUBLES, 0), (11, DOUBLES, 1), (14, (7,), 0), (15, (7,), 1))
+    tasks = ((0, 0, 1), (1, 0, 2), (2, 0, 3), (4, 1, 0), (5, 1, 1), (6, 1, 2), (7, 1, 3),
+             (9, 2, 0), (10, 2, 1), (11, 2, 2), (12, 2, 3))
 
     def unit(n, carry):
-        for start, rels, gz_static in groups:
+        for start, level, i in tasks:
 
             @pl.when(n == start)
             def _():
-                received(rels, gz_static)
+                received(level, i)
 
         third = (n + 1) % 3
-        gz = jnp.where(n < 2, n, jnp.where(n < 14, ((n - 2) // 3) % 2, n - 14))
+        turn = jnp.where(n < 2, n, jnp.where(n < 14, ((n - 2) // 3) % 2, n - 14))
+        gz = (turn + me.g[1]) % 2
         single = jnp.where(third == 0, 1, jnp.where(third == 1, 2, 4))
         double = jnp.where(third == 0, 3, jnp.where(third == 1, 5, 6))
         rel = jnp.where(n < 2, 0, jnp.where(n < 8, single, jnp.where(n < 14, double, 7)))
@@ -263,14 +321,23 @@
             s_own = tile_at(j, 0, me.tp)
             whole = (gz < gz_q) | (same & far & ((me.a[0] + gz) % 2 == 1))
 
-            @pl.when(whole)
+            near = same & jnp.logical_not(far)
+            upper_q = j % 2 == 1
+            side = (rel // 2) % 2 == 1
+            fits = (me.a[1] + j % 2) % 2 == 1
+
+            @pl.when(whole | (near & side & upper_q & fits))
             def _():
                 tiles_step(tiles, j)
 
-            @pl.when(same & jnp.logical_not(far))
+            @pl.when(near & ((side & (upper_q != fits)) | (jnp.logical_not(side) & upper_q)))
+            def _():
+                tiles_step(tiles[0:2], j)
+
+            @pl.when(near & jnp.logical_not(side))
             def _():
                 def one(i, c):
-                    t = sp_of(a_there, (gz, i // 2, i % 2))
+                    t = sp_of(a_there, (gz, j % 2, i))
 
                     @pl.when(t < s_own)
                     def _():
@@ -278,7 +345,7 @@
 
                     return c
 
-                lax.fori_loop(0, 4, one, 0)
+                lax.fori_loop(0, 2, one, 0)
 
             return inner
 
@@ -428,32 +495,10 @@
         both = jnp.dot(blend[...], column, preferred_element_type=f32)
         out_ref[:, at] = (after[:, at].astype(f32) + (both[0:128] + both[128:256])).astype(bf16)
 
-    for j in range(4):
-        chip = tile_at(j, 0, me.tp)
-        for b in range(2):
-
-            @pl.when(jnp.logical_not((chip == me.sp) & (me.tp == b)))
-            def _():
-                arrival(att_send.at[j, b], att_ssem.at[j, b])
-
-        for rel in range(8):
-            if rel:
-                arrival(kv_all.at[tile_at(j, 0, me.tp)], s2_send.at[j, rel])
-            arrival(kv_all.at[tile_at(j, rel, me.tp)], sib_send.at[j, rel])
-    for hl in range(4):
-        chip = sp_of(me.a, (me.tp, hl // 2, hl % 2))
-
-        @pl.when(jnp.logical_not((chip == me.sp) & (me.parity == me.tp)))
-        def _():
-            for n, src in enumerate((kv_own, q_own, lam_own)):
-                arrival(src.at[hl], s1_send.at[n, hl])
-
-    @pl.loop(0, 64)
-    def _(i):
-        @pl.when(i != me.sp)
-        def _():
-            arrival(out_buf.at[i], d_send.at[i])
-            arrival(ret_buf.at[i], r_send.at[i])
+    drain_heads()
+    drain_keys()
+    drain_rows(out_buf, d_send)
+    drain_rows(ret_buf, r_send)
 
 
 def on_device(

time: 146 us -> 138 us (0.945); the launches traced: 146 us -> 135 us
  Pallas kernels: 144 us -> 133 us
    pallas_call x1, Pallas kernels: 144 us -> 133 us  [on_device(): pl.pallas_call(layer_kernel, out_shape=jax.ShapeDtypeStruct(residual.shap...]
where the time goes in v3:
time: 138 us; the launch traced here: 135 us
  Pallas kernels  133 us (96%)
  local copies, waits for them, and re-layouts  1.88 us (1%)
    pallas_call x1, Pallas kernels, on_device(): pl.pallas_call(layer_kernel, out_shape=jax.ShapeDtypeStruct(residual.shap...  133 us

profile of v3, /device:TPU:2, one launch (start us, length us, event | category | flops | bytes accessed | tf_op | source)
XLA Modules:
  0.0 135.1 jit_solution(2961888991436355446)
XLA Ops:
  0.0 133.2 %layer.1 = bf16[128,2048]{1,0:T(8,128)(2,1)} custom-call(bf16[256,256]{1,0:T(8,128)(2,1)} %q1_in.1, bf16[256,256]{1,0:T(8,128)(2,1)} %k1_in.1, bf16[256,256]{1,0:T(8,128)(2,1)} %q2_in.1, bf16[256,256]{1,0:T(8,128)(2,1)} %k2_in.1, bf16[256,512]{1,0:T(8,128)(2,1)} %v_in.1, f32[4]{0:T(128)} %lam_in.1, f32[1,128]{1,0:T(1,128)} %bitcast.7, ...), custom_call_target="tpu_custom_call" | custom-call | tf_op jit(solution)/shard_map/layer/pallas_call | solution.py:513
  133.2 1.9 %copy.17 = bf16[128,2048]{1,0:T(8,128)(2,1)} copy(bf16[128,2048]{1,0:T(8,128)(2,1)} %layer.1) | data formatting | bytes 1048576

commit v4 on v3

--- a/solution.py
+++ b/solution.py
@@ -295,6 +295,37 @@
     tasks = ((0, 0, 1), (1, 0, 2), (2, 0, 3), (4, 1, 0), (5, 1, 1), (6, 1, 2), (7, 1, 3),
              (9, 2, 0), (10, 2, 1), (11, 2, 2), (12, 2, 3))
 
+    def pair_step(tiles, first):
+        second = first + 1
+        m = jnp.concatenate([m_ref[first], m_ref[second]], axis=1)
+        l = jnp.concatenate([l_ref[first], l_ref[second]], axis=1)
+        queries = jnp.concatenate([q_wide[first], q_wide[second]], axis=1)
+        groups_here = [tiles[i : i + 2] for i in range(0, len(tiles), 2)]
+
+        def scores(group):
+            keys = jnp.concatenate([kv_all[t, 0:256, :] for t in group], axis=0)
+            return jnp.dot(keys, queries, preferred_element_type=f32)
+
+        s = scores(groups_here[0])
+        for i, group in enumerate(groups_here):
+            following = scores(groups_here[i + 1]) if i + 1 < len(groups_here) else None
+            newest = jnp.maximum(m, jnp.max(s, axis=0, keepdims=True))
+            p = jnp.exp(s - newest).astype(bf16)
+            factor = jnp.exp(m - newest)
+            values = jnp.concatenate(
+                [kv_all[t, 256 + 128 * b : 384 + 128 * b, :] for t in group for b in range(2)], axis=1
+            )
+            values = jnp.concatenate([values, jnp.ones((16, values.shape[1]), bf16)], axis=0)
+            product = jnp.dot(values, p, preferred_element_type=f32)
+            l = l * factor + product[128:129]
+            acc[first] = acc[first] * factor[:, 0:512] + product[0:128, 0:512]
+            acc[second] = acc[second] * factor[:, 512:1024] + product[0:128, 512:1024]
+            m, s = newest, following
+        m_ref[first] = m[:, 0:512]
+        m_ref[second] = m[:, 512:1024]
+        l_ref[first] = l[:, 0:512]
+        l_ref[second] = l[:, 512:1024]
+
     def unit(n, carry):
         for start, level, i in tasks:
 
@@ -315,18 +346,26 @@
         tiles = [sp_of(a_there, (gz, y, x)) for y in range(2) for x in range(2)]
         far = rel // 4 == 1
 
-        def one_query(j, inner):
-            gz_q = j // 2
-            same = gz_q == gz
+        def two_queries(k, inner):
+            needed = jnp.where(k == 0, gz == 0, far & ((me.a[0] + gz) % 2 == 1))
+
+            @pl.when(needed)
+            def _():
+                pair_step(tiles, jnp.where(k == 0, 2, 2 * gz))
+
+            return inner
+
+        lax.fori_loop(0, 2, two_queries, 0)
+
+        def one_query(upper_q, inner):
+            j = 2 * gz + upper_q
+            upper_q = upper_q == 1
             s_own = tile_at(j, 0, me.tp)
-            whole = (gz < gz_q) | (same & far & ((me.a[0] + gz) % 2 == 1))
-
-            near = same & jnp.logical_not(far)
-            upper_q = j % 2 == 1
+            near = jnp.logical_not(far)
             side = (rel // 2) % 2 == 1
             fits = (me.a[1] + j % 2) % 2 == 1
 
-            @pl.when(whole | (near & side & upper_q & fits))
+            @pl.when(near & side & upper_q & fits)
             def _():
                 tiles_step(tiles, j)
 
@@ -349,16 +388,16 @@
 
             return inner
 
-        return lax.fori_loop(0, 4, one_query, carry)
+        return lax.fori_loop(0, 2, one_query, carry)
 
     lax.fori_loop(0, 16, unit, 0)
 
     def finish(j, carry):
-        total = acc[j] / l_ref[j]
+        inverse = 1.0 / l_ref[j]
+        lam = lam_all[0, 0:1, :]
         for b in range(2):
-            first = total[:, 128 * b : 128 * b + 128]
-            second = total[:, 256 + 128 * b : 384 + 128 * b]
-            out = first - lam_all[0, 0:1, :] * second
+            at_one, at_two = slice(128 * b, 128 * b + 128), slice(256 + 128 * b, 384 + 128 * b)
+            out = acc[j, :, at_one] * inverse[:, at_one] - acc[j, :, at_two] * (lam * inverse[:, at_two])
             mean = jnp.mean(out * out, axis=0, keepdims=True)
             out = (out * lax.rsqrt(mean + epsilon)).T * gain_in[...]
             att_send[j, b] = out.astype(bf16)
@@ -425,9 +464,14 @@
             columns.append(jnp.concatenate(pieces, axis=0))
         return jnp.concatenate(columns, axis=1)
 
-    def block_of(step):
-        shift = jnp.where(step == 2, 3, jnp.where(step == 3, 2, step))
-        return (me.z + shift) % 4
+    def turn_of(step):
+        return jnp.where(step == 0, 0, jnp.where(step == 1, 1, jnp.where(step == 2, 3, 2)))
+
+    def block_to(step):
+        return (me.z + turn_of(step)) % 4
+
+    def block_from(step):
+        return (me.z + 4 - turn_of(step)) % 4
 
     def spread(blk, source, target, ssem, rsem):
         def one(i, carry):
@@ -453,7 +497,7 @@
         lax.fori_loop(0, 16, one, 0)
 
     def dispatch(step, carry):
-        blk = block_of(step)
+        blk = block_to(step)
         rows = pl.ds(pl.multiple_of(blk * 128, 128), 128)
         value = jnp.dot(pick[rows, :], routed[...], preferred_element_type=f32).astype(bf16)
         packed(value, out_buf, blk)
@@ -468,7 +512,7 @@
         c.wait()
 
     def work(step, carry):
-        blk = block_of(step)
+        blk = block_from(step)
         collect(blk, arr_buf, d_recv)
         x = unpacked(arr_buf, blk, False)
         hidden = []

time: 138 us -> 128 us (0.928)
  Pallas kernels: 133 us -> 124 us
    pallas_call x1, Pallas kernels: 133 us -> 124 us  [on_device(): pl.pallas_call(layer_kernel, out_shape=jax.ShapeDtypeStruct(residual.shap...]
where the time goes in v4:
time: 128 us; the launch traced here: 126 us
  Pallas kernels  124 us (97%)
  local copies, waits for them, and re-layouts  1.88 us (1%)
    pallas_call x1, Pallas kernels, on_device(): pl.pallas_call(layer_kernel, out_shape=jax.ShapeDtypeStruct(residual.shap...  124 us

profile of v4, /device:TPU:2, one launch (start us, length us, event | category | flops | bytes accessed | tf_op | source)
XLA Modules:
  0.0 126.3 jit_solution(12417998299586339642)
XLA Ops:
  0.0 124.4 %layer.1 = bf16[128,2048]{1,0:T(8,128)(2,1)} custom-call(bf16[256,256]{1,0:T(8,128)(2,1)} %q1_in.1, bf16[256,256]{1,0:T(8,128)(2,1)} %k1_in.1, bf16[256,256]{1,0:T(8,128)(2,1)} %q2_in.1, bf16[256,256]{1,0:T(8,128)(2,1)} %k2_in.1, bf16[256,512]{1,0:T(8,128)(2,1)} %v_in.1, f32[4]{0:T(128)} %lam_in.1, f32[1,128]{1,0:T(1,128)} %bitcast.7, ...), custom_call_target="tpu_custom_call" | custom-call | tf_op jit(solution)/shard_map/layer/pallas_call | solution.py:557
  124.4 1.9 %copy.17 = bf16[128,2048]{1,0:T(8,128)(2,1)} copy(bf16[128,2048]{1,0:T(8,128)(2,1)} %layer.1) | data formatting | bytes 1048576

commit v5 on v4

--- a/solution.py
+++ b/solution.py
@@ -265,7 +265,7 @@
         return carry
 
     received(0, 0)
-    lax.fori_loop(0, 4, diagonal, 0)
+    lax.fori_loop(0, 4, diagonal, 0, unroll=2)
 
     def tiles_step(tiles, j):
         m, l = m_ref[j], l_ref[j]
@@ -432,7 +432,7 @@
         value = value.astype(f32)
         return square + jnp.sum(value * value, axis=1, keepdims=True)
 
-    square = lax.fori_loop(0, 4, project, jnp.zeros((128, 1), f32))
+    square = lax.fori_loop(0, 4, project, jnp.zeros((128, 1), f32), unroll=4)
     inverse = lax.rsqrt(square * (1.0 / WIDTH) + epsilon)
 
     def norm(n, carry):
@@ -440,7 +440,7 @@
         routed[:, at] = (after[:, at].astype(f32) * inverse * ng_in[:, at]).astype(bf16)
         return carry
 
-    lax.fori_loop(0, 4, norm, 0)
+    lax.fori_loop(0, 4, norm, 0, unroll=4)
 
     def packed(value, into, blk):
         rows = pl.ds(pl.multiple_of(blk * 256, 256), 256)

time: 128 us -> 133 us (1.039)
  the two profiles are of different devices: /device:TPU:2 before, /device:TPU:74 now
where the time goes in v5:
time: 133 us
  Pallas kernels  131 us (98%)
  local copies, waits for them, and re-layouts  1.88 us (1%)
    pallas_call x1, Pallas kernels, on_device(): pl.pallas_call(layer_kernel, out_shape=jax.ShapeDtypeStruct(residual.shap...  131 us

profile of v5, /device:TPU:74, one launch (start us, length us, event | category | flops | bytes accessed | tf_op | source)
XLA Modules:
  0.0 132.8 jit_solution(13827747892556532587)
XLA Ops:
  0.0 130.9 %layer.1 = bf16[128,2048]{1,0:T(8,128)(2,1)} custom-call(bf16[256,256]{1,0:T(8,128)(2,1)} %q1_in.1, bf16[256,256]{1,0:T(8,128)(2,1)} %k1_in.1, bf16[256,256]{1,0:T(8,128)(2,1)} %q2_in.1, bf16[256,256]{1,0:T(8,128)(2,1)} %k2_in.1, bf16[256,512]{1,0:T(8,128)(2,1)} %v_in.1, f32[4]{0:T(128)} %lam_in.1, f32[1,128]{1,0:T(1,128)} %bitcast.7, ...), custom_call_target="tpu_custom_call" | custom-call | tf_op jit(solution)/shard_map/layer/pallas_call | solution.py:557
  130.9 1.9 %copy.17 = bf16[128,2048]{1,0:T(8,128)(2,1)} copy(bf16[128,2048]{1,0:T(8,128)(2,1)} %layer.1) | data formatting | bytes 1048576
